TPU v7x, 32 devices: a whole 2x2x4 slice. The times are simulated.
32 devices in a mesh: ep: 4 (over y, x), tp: 8 (over z, core).
Axes of the slice: x: 2, y: 2, z: 4, core: 2. Of those that a mesh axis runs over, the one named last changes fastest.
Arguments:
- tokens: bfloat16 [64, 4096], P('ep'), may hold values from -150 to 150
- query_weight: bfloat16 [4096, 1024], P('tp'), may hold values from -0.09375 to 0.09375
- key_weight: bfloat16 [4096, 1024], P('tp'), may hold values from -0.09375 to 0.09375
- value_weight: bfloat16 [4096, 2048], P(None, 'tp'), may hold values from -0.09375 to 0.09375
- decay_down: bfloat16 [4096, 16], replicated, may hold values from -0.09375 to 0.09375
- decay_up: float32 [16, 1024], replicated, may hold values from -3 to 3
- decay_bias: float32 [1024], replicated, may hold values from -8 to 4
- old_state: float32 [64, 256, 2048], P('ep', None, 'tp'), may hold values from -8 to 8
- out_weight: bfloat16 [2048, 4096], P('tp'), may hold values from -0.1875 to 0.1875
- norm_gain: float32 [4096], replicated, may hold values from 0.2 to 4
- router_weight: bfloat16 [4096, 4], replicated, may hold values from -0.09375 to 0.09375
- routing: int32 [64, 2], P('ep'), may hold values from 0 to 3, all different within a row; in each aligned block of 16 rows (0 to 15, 16 to 31, ...) at most 16 rows name the same one
- glu_weight: bfloat16 [4, 4096, 2048], P('ep', None, 'tp'), may hold values from -0.25 to 0.25
- linear_weight: bfloat16 [4, 4096, 2048], P('ep', None, 'tp'), may hold values from -0.25 to 0.25
- down_weight: bfloat16 [4, 2048, 4096], P('ep', 'tp'), may hold values from -0.01953125 to 0.01953125
- final_gain: float32 [4096], replicated, may hold values from 0.1 to 1.9
Outputs:
- layer_out: bfloat16 [64, 4096], P('ep', 'tp')
- new_state: float32 [64, 256, 2048], P('ep', None, 'tp')
Inputs may be any that keep to these rules, and one draw needn't show every extreme that they name: `routing`: within the rows of one device (aligned blocks of 16 rows) no expert is named by more than 16 rows, and at least one block reaches that bound; each row names 2 different experts.
All inputs are finite; a program needn't handle non-finite values.
Results may differ from a plain program's by a relative error of at most 0.015.
Values may be sent and summed in bfloat16 or wider, within the bound.
A program may use at most 64 MiB of HBM per device.

v0:
```python
import jax
import jax.numpy as jnp
from jax import lax
from jax.sharding import PartitionSpec as P

ALPHA = 2.0**0.25
TAU = 16.0
LIMIT = 7.0
SLOPE = 1.702
EPSILON = 1e-05


def norm_from_totals(inputs, totals, width, gain):
    mean = totals[0][:, None] / width
    variance = totals[1][:, None] / width - mean * mean
    return (inputs - mean) * lax.rsqrt(variance + EPSILON) * gain


def row_totals(inputs):
    return (jnp.sum(inputs, axis=1), jnp.sum(inputs * inputs, axis=1))


def clamped_unit(glu_pre, linear_pre):
    glu = jnp.minimum(glu_pre, LIMIT)
    linear = jnp.clip(linear_pre, -LIMIT, LIMIT)
    return glu * jax.nn.sigmoid(SLOPE * glu) * (linear + 1.0)


def expert_gate(logits, slot_ids, own_expert):
    expert_ids = jnp.arange(logits.shape[1], dtype=jnp.int32)
    picked = jnp.sum(
        jnp.where(slot_ids[:, :, None] == expert_ids[None, None, :], logits[:, None, :], 0.0),
        axis=2,
    )
    own_logit = jnp.sum(jnp.where(expert_ids[None, :] == own_expert, logits, 0.0), axis=1)
    return jnp.exp(own_logit) / jnp.sum(jnp.exp(picked), axis=1)


def per_device(
    tokens,
    query_weight,
    key_weight,
    value_weight,
    decay_down,
    decay_up,
    decay_bias,
    old_state,
    out_weight,
    norm_gain,
    router_weight,
    routing,
    glu_weight,
    linear_weight,
    down_weight,
    final_gain,
):
    tp_count = lax.axis_size("tp")
    tp_rank = lax.axis_index("tp")
    own_expert = lax.axis_index("ep")
    seq_count, width = tokens.shape
    head_dk = old_state.shape[1]
    heads = query_weight.shape[1] // head_dk
    head_start = tp_rank // (tp_count // heads) * head_dk
    top_count = routing.shape[1]
    experts = router_weight.shape[1]
    slot_cap = max(2, (2 * seq_count * top_count + experts - 1) // experts)
    share_width = width // tp_count
    share_start = tp_rank * share_width
    glu_local = glu_weight[0]
    linear_local = linear_weight[0]
    down_local = down_weight[0]
    token_share = lax.dynamic_slice_in_dim(tokens, share_start, share_width, 1)
    query_part = jnp.dot(token_share, query_weight, preferred_element_type=jnp.float32)
    key_part = jnp.dot(token_share, key_weight, preferred_element_type=jnp.float32)
    query_sum, key_sum = lax.psum((query_part, key_part), "tp")
    query_all = query_sum.astype(jnp.bfloat16)
    key_all = key_sum.astype(jnp.bfloat16)
    values = jnp.dot(tokens, value_weight, preferred_element_type=jnp.float32).astype(jnp.bfloat16)
    low_rank = jnp.dot(tokens, decay_down, preferred_element_type=jnp.float32)
    up_cols = lax.dynamic_slice_in_dim(decay_up, head_start, head_dk, 1)
    bias_cols = lax.dynamic_slice_in_dim(decay_bias, head_start, head_dk, 0)
    decay = jnp.exp(
        jax.nn.log_sigmoid(jnp.dot(low_rank, up_cols, precision=lax.Precision.HIGHEST) + bias_cols)
        / TAU
    )
    query = lax.dynamic_slice_in_dim(query_all, head_start, head_dk, 1).astype(jnp.float32)
    keys = lax.dynamic_slice_in_dim(key_all, head_start, head_dk, 1).astype(jnp.float32)
    new_state = (
        decay[:, :, None] * old_state + keys[:, :, None] * values.astype(jnp.float32)[:, None, :]
    )
    mixed = (
        jnp.einsum("si,sic->sc", query, new_state, precision=lax.Precision.HIGHEST)
        * head_dk ** (-0.5)
    ).astype(jnp.bfloat16)
    out_terms = jnp.dot(mixed, out_weight, preferred_element_type=jnp.float32)
    flat_ids = routing.reshape(-1)
    expert_ids = jnp.arange(experts, dtype=jnp.int32)
    chosen = (flat_ids[:, None] == expert_ids[None, :]).astype(jnp.int32)
    before = jnp.cumsum(chosen, axis=0) - chosen
    slot_rank = jnp.sum(before * chosen, axis=1)
    slot_index = flat_ids * slot_cap + slot_rank
    placed = (
        slot_index[:, None] == jnp.arange(experts * slot_cap, dtype=jnp.int32)[None, :]
    ).astype(jnp.int32)
    spread = jnp.sum(placed.reshape(seq_count, top_count, experts * slot_cap), axis=1)
    spread_rows = spread.astype(jnp.bfloat16)
    slot_ids = jnp.einsum("sn,sk->nk", spread, routing).reshape(experts, slot_cap, top_count)
    projected = lax.psum_scatter(out_terms, "tp", scatter_dimension=1, tiled=True)
    hidden_in = ALPHA * token_share.astype(jnp.float32) + projected
    first = lax.psum(row_totals(hidden_in), "tp")
    gain_share = lax.dynamic_slice_in_dim(norm_gain, share_start, share_width, 0)
    normed = norm_from_totals(hidden_in, first, width, gain_share).astype(jnp.bfloat16)
    send_rows = jnp.einsum(
        "sn,sd->nd", spread_rows, normed, preferred_element_type=jnp.float32
    ).astype(jnp.bfloat16)
    send_rows = send_rows.reshape(experts, slot_cap, normed.shape[1])
    rows_in = lax.all_to_all(send_rows, "ep", split_axis=0, concat_axis=0, tiled=True)
    ids_in = lax.all_to_all(slot_ids, "ep", split_axis=0, concat_axis=0, tiled=True)
    sources, slots, row_width = rows_in.shape
    count = sources * slots
    piece = lax.all_gather(rows_in, "tp", axis=2, tiled=True)
    size = piece.shape[2]
    flat = piece.reshape(count, size)
    glu_pre = jnp.dot(flat, glu_local, preferred_element_type=jnp.float32)
    linear_pre = jnp.dot(flat, linear_local, preferred_element_type=jnp.float32)
    logits = jnp.dot(flat, router_weight, preferred_element_type=jnp.float32)
    act = clamped_unit(glu_pre, linear_pre).astype(jnp.bfloat16)
    summed = lax.psum_scatter(
        jnp.dot(act, down_local, preferred_element_type=jnp.float32),
        "tp",
        scatter_dimension=1,
        tiled=True,
    )
    gate = expert_gate(logits, ids_in.reshape(count, top_count), own_expert)
    weighted = (
        (summed * gate[:, None]).astype(jnp.bfloat16).reshape(sources, slots, summed.shape[1])
    )
    returned = lax.all_to_all(weighted, "ep", split_axis=0, concat_axis=0, tiled=True)
    combined = ALPHA * normed.astype(jnp.float32) + jnp.einsum(
        "sn,nd->sd",
        spread_rows,
        returned.reshape(experts * slot_cap, normed.shape[1]),
        preferred_element_type=jnp.float32,
    )
    second = lax.psum(row_totals(combined), "tp")
    final_share = lax.dynamic_slice_in_dim(final_gain, share_start, share_width, 0)
    layer_out = norm_from_totals(combined, second, width, final_share).astype(jnp.bfloat16)
    return (layer_out, new_state)


def solution(mesh):
    return jax.shard_map(
        per_device,
        mesh=mesh,
        in_specs=(
            P("ep", None),
            P("tp", None),
            P("tp", None),
            P(None, "tp"),
            P(),
            P(),
            P(),
            P("ep", None, "tp"),
            P("tp", None),
            P(),
            P(),
            P("ep", None),
            P("ep", None, "tp"),
            P("ep", None, "tp"),
            P("ep", "tp", None),
            P(),
        ),
        out_specs=(P("ep", "tp"), P("ep", None, "tp")),
        check_vma=False,
    )
```

profile of v0, /device:TPU:0, one launch (start us, length us, event | category | flops | bytes accessed | tf_op | source)
XLA Modules:
  0.0 188.1 jit_solution(6148383914185210825)
XLA Ops:
  7.2 0.0 copy-start
  7.2 0.0 copy-start.3
  7.2 0.0 copy-start.4
  7.2 0.0 reduce-scatter.3.cloned.1.call-start
  7.3 1.6 fusion.43
  8.9 1.5 fusion.45
  10.4 31.6 %all-reduce.4 = (bf16[16,1024]{1,0:T(8,128)(2,1)S(1)}, bf16[16,1024]{1,0:T(8,128)(2,1)S(1)}) all-reduce(f32[16,1024]{1,0:T(8,128)S(1)} %fusion.43, f32[16,1024]{1,0:T(8,128)S(1)} %fusion.45), channel_id=1, replica_groups=mesh['ep'=4,'tp'=8] {'tp'}, use_global_device_ids=true, to_apply=%region_1.2 | all-reduce | flops 32768 | bytes 196608 | tf_op jit(solution)/shard_map/psum | solution.py:75
  42.0 0.8 dynamic_slice.24
  42.8 0.0 copy-done.3
  42.8 0.0 copy-done.4
  42.8 0.2 fusion.66
  42.9 2.0 %fusion.24 = f32[16,256]{1,0:T(8,128)S(1)} fusion(bf16[16,4096]{1,0:T(8,128)(2,1)S(1)} %copy-done.3, bf16[4096,256]{1,0:T(8,128)(2,1)} %param.19), kind=kOutput, calls=%fused_computation.17 | convolution fusion | flops 33562624 | bytes 2244608 | tf_op jit(solution)/shard_map/dot_general | solution.py:78
  44.9 0.9 fusion.37
  45.8 2.9 %multiply_add_fusion = f32[16,256,256]{2,1,0:T(8,128)S(1)} fusion(f32[16,256,256]{2,1,0:T(8,128)} %param.23, f32[16,256]{1,0:T(8,128)S(1)} %fusion.24, f32[16,256]{1,0:T(8,128)S(1)} %fusion.50, f32[16,256]{1,0:T(8,128)S(1)} %fusion.37), kind=kLoop, calls=%fused_computation | loop fusion | flops 3145728 | bytes 8437760 | tf_op jit(solution)/shard_map/add | solution.py:89
  48.7 0.0 copy-start.1
  48.7 0.0 copy-start.2
  48.7 1.5 fusion.39
  50.2 0.6 copy-done.1
  50.8 1.0 copy-done.2
  51.8 0.0 copy-start.5
  51.8 1.1 fusion.47
  52.9 0.0 reduce-scatter.3.cloned.1.call-update
  52.9 0.0 reduce-scatter.5.cloned.1.call-start
  53.0 0.0 copy-done.5
  53.0 0.1 copy.36
  53.1 0.1 eq.55
  53.1 0.1 fusion.41
  53.2 0.8 dynamic_slice.26
  54.0 0.1 reduce_window_sum.11
  54.0 0.2 select_reduce_fusion
  54.2 0.1 reduce_sum.86
  54.3 0.1 copy.37
  54.4 0.1 convert_reduce_fusion
  54.5 27.6 %reduce-scatter.3.cloned.1.call-done = f32[16,512]{1,0:T(8,128)} async-done(((f32[16,4096]{1,0:T(8,128)}), f32[16,512]{1,0:T(8,128)}) %reduce-scatter.3.cloned.1.call-update) | async-done | bytes 32784 | tf_op jit(solution)/shard_map/reduce_scatter | solution.py:108
  82.1 0.9 fusion.52
  83.0 13.7 %all-reduce.1 = (f32[16]{0:T(128)S(1)}, f32[16]{0:T(128)S(1)}) all-reduce(f32[16]{0:T(128)S(1)} %get-tuple-element.3, f32[16]{0:T(128)S(1)} %get-tuple-element.2), channel_id=1, replica_groups=mesh['ep'=4,'tp'=8] {'tp'}, use_global_device_ids=true, to_apply=%region_6.7 | all-reduce | flops 32 | bytes 256 | tf_op jit(solution)/shard_map/psum | solution.py:110
  96.7 0.8 multiply_convert_fusion.2
  97.6 0.2 convolution_convert_fusion
  97.7 8.5 %all_to_all.15 = bf16[4,16,512]{2,1,0:T(8,128)(2,1)S(1)} all-to-all(bf16[4,16,512]{2,1,0:T(8,128)(2,1)S(1)} %bitcast.58), channel_id=1, replica_groups=mesh['ep'=4,'tp'=8] {'ep'}, dimensions={0} | all-to-all | bytes 131072 | tf_op jit(solution)/shard_map/all_to_all | solution.py:117
  106.3 14.9 %all_gather.3 = bf16[4,16,4096]{2,1,0:T(8,128)(2,1)S(1)} all-gather(bf16[4,16,512]{2,1,0:T(8,128)(2,1)S(1)} %all_to_all.15), channel_id=1, replica_groups=mesh['ep'=4,'tp'=8] {'tp'}, dimensions={2}, use_global_device_ids=true | all-gather | bytes 589824 | tf_op jit(solution)/shard_map/all_gather | solution.py:121
  121.2 2.0 %fusion.6 = f32[64,256]{1,0:T(8,128)S(1)} fusion(bf16[64,4096]{1,0:T(8,128)(2,1)S(1)} %bitcast.55, bf16[1,4096,256]{2,1,0:T(8,128)(2,1)} %param.28), kind=kOutput, calls=%fused_computation.8 | convolution fusion | flops 134234112 | bytes 2686976 | tf_op jit(solution)/shard_map/dot_general | solution.py:124
  123.3 0.0 copy-done
  123.3 0.0 copy-start.6
  123.3 4.0 %fusion = f32[64,4096]{1,0:T(8,128)} fusion(bf16[1,256,4096]{2,1,0:T(8,128)(2,1)S(1)} %copy-done, bf16[64,4096]{1,0:T(8,128)(2,1)S(1)} %bitcast.56, bf16[1,4096,256]{2,1,0:T(8,128)(2,1)} %param.29, f32[64,256]{1,0:T(8,128)S(1)} %fusion.6), kind=kOutput, calls=%fused_computation.1 | convolution fusion | flops 268582912 | bytes 5832704 | tf_op jit(solution)/shard_map/dot_general | solution.py:129
  127.3 0.0 reduce-scatter.5.cloned.1.call-update
  127.3 0.1 copy.42
  127.4 1.1 fusion.55
  128.5 3.2 %all-to-all-start.1 = ((s32[4,16,2]{1,2,0:T(2,128)}), s32[4,16,2]{1,2,0:T(2,128)S(1)}, u32[]{:S(2)}, u32[]{:S(2)}) async-start(s32[4,16,2]{1,2,0:T(2,128)} %fusion.55), calls=%async_computation.3 | async-start | bytes 8192 | tf_op jit(solution)/shard_map/all_to_all | solution.py:118
  131.7 4.6 %all-to-all-done.1 = s32[4,16,2]{1,2,0:T(2,128)S(1)} async-done(((s32[4,16,2]{1,2,0:T(2,128)}), s32[4,16,2]{1,2,0:T(2,128)S(1)}, u32[]{:S(2)}, u32[]{:S(2)}) %all-to-all-start.1) | async-done | bytes 544 | tf_op jit(solution)/shard_map/all_to_all | solution.py:118
  136.4 0.1 eq.64
  136.5 0.0 copy-done.6
  136.5 0.3 select_reduce_fusion.2
  136.8 19.8 %reduce-scatter.5.cloned.1.call-done = f32[64,512]{1,0:T(8,128)} async-done(((f32[64,4096]{1,0:T(8,128)}), f32[64,512]{1,0:T(8,128)}) %reduce-scatter.5.cloned.1.call-update) | async-done | bytes 131088 | tf_op jit(solution)/shard_map/reduce_scatter | solution.py:128
  156.6 1.6 multiply_convert_fusion
  158.2 3.7 %all-to-all-start.2 = ((bf16[4,16,512]{2,1,0:T(8,128)(2,1)}), bf16[4,16,512]{2,1,0:T(8,128)(2,1)S(1)}, u32[]{:S(2)}, u32[]{:S(2)}) async-start(bf16[4,16,512]{2,1,0:T(8,128)(2,1)} %bitcast.10), calls=%async_computation.4 | async-start | bytes 131072 | tf_op jit(solution)/shard_map/all_to_all | solution.py:138
  161.9 0.8 dynamic_slice.27
  162.7 4.1 %all-to-all-done.2 = bf16[4,16,512]{2,1,0:T(8,128)(2,1)S(1)} async-done(((bf16[4,16,512]{2,1,0:T(8,128)(2,1)}), bf16[4,16,512]{2,1,0:T(8,128)(2,1)S(1)}, u32[]{:S(2)}, u32[]{:S(2)}) %all-to-all-start.2) | async-done | bytes 65568 | tf_op jit(solution)/shard_map/all_to_all | solution.py:138
  166.8 0.2 fusion.65
  167.0 13.6 %all-reduce = (f32[16]{0:T(128)S(1)}, f32[16]{0:T(128)S(1)}) all-reduce(f32[16]{0:T(128)S(1)} %get-tuple-element.5, f32[16]{0:T(128)S(1)} %get-tuple-element.4), channel_id=1, replica_groups=mesh['ep'=4,'tp'=8] {'tp'}, use_global_device_ids=true, to_apply=%region_17.18 | all-reduce | flops 32 | bytes 256 | tf_op jit(solution)/shard_map/psum | solution.py:145
  180.6 0.7 multiply_convert_fusion.1
  (10 shorter events, 0.1 us)
Async XLA Ops:
  7.2 116.1 %copy-start = (bf16[1,256,4096]{2,1,0:T(8,128)(2,1)S(1)}, bf16[1,256,4096]{2,1,0:T(8,128)(2,1)}, u32[]{:S(2)}) copy-start(bf16[1,256,4096]{2,1,0:T(8,128)(2,1)} %param.30) | copy-start | bytes 6291460
  7.2 35.6 %copy-start.3 = (bf16[16,4096]{1,0:T(8,128)(2,1)S(1)}, bf16[16,4096]{1,0:T(8,128)(2,1)}, u32[]{:S(2)}) copy-start(bf16[16,4096]{1,0:T(8,128)(2,1)} %param.16) | copy-start | bytes 393220
  7.2 35.6 %copy-start.4 = (bf16[4096,16]{0,1:T(8,128)(2,1)S(1)}, bf16[4096,16]{0,1:T(8,128)(2,1)}, u32[]{:S(2)}) copy-start(bf16[4096,16]{0,1:T(8,128)(2,1)} %param.20) | copy-start | bytes 393220
  7.2 74.9 %reduce-scatter.3.cloned.1.call-start = ((), (), s32[]{:S(2)}) async-start(), calls=%async_computation.5 | async-start | bytes 294912 | tf_op jit(solution)/shard_map/reduce_scatter | solution.py:108
  48.7 2.1 %copy-start.1 = (f32[16,256,256]{2,1,0:T(8,128)}, f32[16,256,256]{2,1,0:T(8,128)S(1)}, u32[]{:S(2)}) copy-start(f32[16,256,256]{2,1,0:T(8,128)S(1)} %multiply_add_fusion) | copy-start | bytes 12582916
  48.7 3.1 %copy-start.2 = (bf16[256,4096]{1,0:T(8,128)(2,1)S(1)}, bf16[256,4096]{1,0:T(8,128)(2,1)}, u32[]{:S(2)}) copy-start(bf16[256,4096]{1,0:T(8,128)(2,1)} %param.24) | copy-start | bytes 6291460
  51.8 1.2 copy-start.5
  52.9 103.7 %reduce-scatter.5.cloned.1.call-start = ((), (), s32[]{:S(2)}) async-start(), calls=%async_computation.6 | async-start | bytes 1179648 | tf_op jit(solution)/shard_map/reduce_scatter | solution.py:128
  123.3 13.2 %copy-start.6 = (bf16[4096,4]{0,1:T(4,128)(2,1)S(1)}, bf16[4096,4]{0,1:T(4,128)(2,1)}, u32[]{:S(2)}) copy-start(bf16[4096,4]{0,1:T(4,128)(2,1)} %param.26) | copy-start | bytes 98308
  128.5 7.9 %all-to-all-start.1 = ((s32[4,16,2]{1,2,0:T(2,128)}), s32[4,16,2]{1,2,0:T(2,128)S(1)}, u32[]{:S(2)}, u32[]{:S(2)}) async-start(s32[4,16,2]{1,2,0:T(2,128)} %fusion.55), calls=%async_computation.3 | async-start | bytes 8192 | tf_op jit(solution)/shard_map/all_to_all | solution.py:118
  158.2 8.6 %all-to-all-start.2 = ((bf16[4,16,512]{2,1,0:T(8,128)(2,1)}), bf16[4,16,512]{2,1,0:T(8,128)(2,1)S(1)}, u32[]{:S(2)}, u32[]{:S(2)}) async-start(bf16[4,16,512]{2,1,0:T(8,128)(2,1)} %bitcast.10), calls=%async_computation.4 | async-start | bytes 131072 | tf_op jit(solution)/shard_map/all_to_all | solution.py:138
Sparse Core Ops, SparseCore 0:
  53.0 28.9 reduce-scatter.2
  127.4 29.1 reduce-scatter.4
where the time goes:
time: 189 us; the launch traced here: 188 us
  blocking collectives  82.4 us (44%)
  waiting for transfers between devices  56.2 us (30%)
  matrix products  16.6 us (9%)
  between operations  14.2 us (8%)
  other arithmetic  7.34 us (4%)
  starting transfers between devices  7.03 us (4%)
  local copies, waits for them, and re-layouts  4.41 us (2%)
    psum x1, blocking collectives, per_device(): query_sum, key_sum = lax.psum((query_part, key_part), 'tp')  31.6 us
    reduce_scatter x1, waiting for transfers between devices, per_device(): lax.psum_scatter(out_terms, 'tp', scatter_dimension=1, tiled=True)  27.6 us
    reduce_scatter x1, waiting for transfers between devices, per_device(): lax.psum_scatter(jnp.dot(act, down_local, preferred_element_type=jnp.floa...  19.8 us
    all_gather x1, blocking collectives, per_device(): piece = lax.all_gather(rows_in, 'tp', axis=2, tiled=True)  14.9 us
    psum x1, blocking collectives, per_device(): first = lax.psum(row_totals(hidden_in), 'tp')  13.7 us
    psum x1, blocking collectives, per_device(): second = lax.psum(row_totals(combined), 'tp')  13.6 us
    all_to_all x1, blocking collectives, per_device(): lax.all_to_all(send_rows, 'ep', split_axis=0, concat_axis=0, tiled=True)  8.53 us
    all_to_all x1, waiting for transfers between devices, per_device(): lax.all_to_all(slot_ids, 'ep', split_axis=0, concat_axis=0, tiled=True)  4.63 us
  transfers between devices with their start and end apart: 4, of which 4 were waited for; matrix products, arithmetic and copies ran while one was open for 2% of the time, Pallas kernels for 0%

commit v1 on v0

v1 whole, which is shorter than its diff:
```python
import functools

import jax
import jax.numpy as jnp
from jax import lax
from jax.experimental import pallas as pl
from jax.experimental.pallas import tpu as pltpu
from jax.sharding import PartitionSpec as P

ALPHA = 2.0**0.25
TAU = 16.0
LIMIT = 7.0
SLOPE = 1.702
EPSILON = 1e-05
MESH = pl.DeviceIdType.MESH
F32 = jnp.float32
BF16 = jnp.bfloat16
MIB = 1 << 20


def mm(a, b):
    return jnp.dot(a, b, preferred_element_type=F32)


def log_sigmoid(z):
    return jnp.minimum(z, 0.0) - jnp.log1p(jnp.exp(-jnp.abs(z)))


def project_kernel(
    tp, heads, dk, tokens, wq, wk, wv, dd, up, bias, pack_out, values_out,
    wq_v, wk_v, wv_v, dd_v, send, recv, load_sem, send_sem, recv_sem,
):
    me = lax.axis_index("tp")
    seqs, width = tokens.shape
    share = width // tp
    group = tp // heads
    loads = [
        pltpu.make_async_copy(src, dst, load_sem.at[i])
        for i, (src, dst) in enumerate(((wq, wq_v), (wk, wk_v), (wv, wv_v), (dd, dd_v)))
    ]
    for load in loads:
        load.start()
    barrier = pltpu.get_barrier_semaphore()

    @pl.loop(1, tp)
    def _(d):
        pl.semaphore_signal(
            barrier, inc=1, device_id={"tp": lax.rem(me + d, tp)}, device_id_type=MESH
        )

    own = tokens[:, pl.ds(pl.multiple_of(me * share, share), share)]
    for i, w in ((0, wq_v), (1, wk_v)):
        loads[i].wait()
        part = mm(own, w[...])
        for h in range(heads):
            send[h, i * seqs : (i + 1) * seqs, :] = part[:, h * dk : (h + 1) * dk].astype(BF16)
    pl.semaphore_wait(barrier, tp - 1)

    def copy_to(peer):
        return pltpu.make_async_remote_copy(
            src_ref=send.at[peer // group],
            dst_ref=recv.at[me],
            send_sem=send_sem.at[peer],
            recv_sem=recv_sem.at[me],
            device_id={"tp": peer},
            device_id_type=MESH,
        )

    def copy_from(peer):
        return pltpu.make_async_remote_copy(
            src_ref=send.at[0],
            dst_ref=recv.at[peer],
            send_sem=send_sem.at[peer],
            recv_sem=recv_sem.at[peer],
            device_id={"tp": peer},
            device_id_type=MESH,
        )

    @pl.loop(1, tp)
    def _(d):
        copy_to(lax.rem(me + d, tp)).start()

    head = me // group
    recv[me] = send[head]
    loads[2].wait()
    values_out[...] = mm(tokens[...], wv_v[...]).astype(BF16).astype(F32)
    loads[3].wait()
    low = mm(tokens[...], dd_v[...])
    cols = pl.ds(pl.multiple_of(head * dk, dk), dk)
    up_cols = up[:, cols]
    z = jnp.broadcast_to(bias[:, cols], (seqs, dk))
    for r in range(low.shape[1]):
        z = z + low[:, r : r + 1] * up_cols[r : r + 1, :]
    decay = jnp.exp(log_sigmoid(z) / TAU)

    @pl.loop(1, tp)
    def _(d):
        copy_from(lax.rem(me + d, tp)).wait_recv()

    total = recv[0].astype(F32)
    for p in range(1, tp):
        total = total + recv[p].astype(F32)
    total = total.astype(BF16).astype(F32)
    pad = pack_out.shape[1] - 3 * seqs
    pack = jnp.concatenate([decay, total, jnp.zeros((pad, dk), F32)], axis=0)
    pack_out[...] = jnp.transpose(pack)

    @pl.loop(1, tp)
    def _(d):
        copy_to(lax.rem(me + d, tp)).wait_send()


def state_kernel(pack, values, old, new, mixed, old_v, new_v, in_sem, out_sem):
    seqs, dk, dv = old_v.shape
    ins = [pltpu.make_async_copy(old.at[s], old_v.at[s], in_sem.at[s]) for s in range(seqs)]
    outs = [pltpu.make_async_copy(new_v.at[s], new.at[s], out_sem.at[s]) for s in range(seqs)]
    for s in range(seqs):
        ins[s].start()
    rows = []
    for s in range(seqs):
        ins[s].wait()
        value = values[s : s + 1, :]
        updated = pack[:, s : s + 1] * old_v[s] + pack[:, 2 * seqs + s : 2 * seqs + s + 1] * value
        new_v[s] = updated
        outs[s].start()
        rows.append(jnp.sum(pack[:, seqs + s : seqs + s + 1] * updated, axis=0, keepdims=True))
    mixed[...] = (jnp.concatenate(rows, axis=0) * dk ** (-0.5)).astype(BF16)
    for s in range(seqs):
        outs[s].wait()


def expert_kernel(
    ep, tp, tokens, mixed, gain, final_gain, routing, wo, router, wg, wl, wd, out,
    wo_v, router_v, wg_v, wl_v, wd_v, b_send, b_recv, rows, normed, d_send, d_recv, stats,
    load_sem, b_ss, b_rs, c_ss, c_rs, d_ss, d_rs, e_ss, e_rs,
):
    e = lax.axis_index("ep")
    t = lax.axis_index("tp")
    n = ep * tp
    me = e * tp + t
    seqs, width = tokens.shape
    share = width // tp
    experts = router_v.shape[1]
    loads = [
        pltpu.make_async_copy(src, dst, load_sem.at[i])
        for i, (src, dst) in enumerate(
            ((wo, wo_v), (wg.at[0], wg_v), (wl.at[0], wl_v), (router, router_v), (wd.at[0], wd_v))
        )
    ]
    for load in loads:
        load.start()
    barrier = pltpu.get_barrier_semaphore()

    def other(d):
        peer = lax.rem(me + d, n)
        return peer, peer // tp, lax.rem(peer, tp)

    @pl.loop(1, n)
    def _(d):
        _, pe, pt = other(d)
        pl.semaphore_signal(barrier, inc=1, device_id={"ep": pe, "tp": pt}, device_id_type=MESH)

    def remote(src, dst, ss, rs, pe, pt):
        return pltpu.make_async_remote_copy(
            src_ref=src, dst_ref=dst, send_sem=ss, recv_sem=rs,
            device_id={"ep": pe, "tp": pt}, device_id_type=MESH,
        )

    loads[0].wait()
    for p in range(tp):
        b_send[p] = mm(mixed[...], wo_v[:, p * share : (p + 1) * share]).astype(BF16)
    pl.semaphore_wait(barrier, n - 1)

    def b_out(p):
        return remote(b_send.at[p], b_recv.at[t], b_ss.at[p], b_rs.at[t], e, p)

    def b_in(p):
        return remote(b_send.at[p], b_recv.at[p], b_ss.at[p], b_rs.at[p], e, p)

    @pl.loop(1, tp)
    def _(d):
        b_out(lax.rem(t + d, tp)).start()

    b_recv[t] = b_send[t]
    share_cols = pl.ds(pl.multiple_of(t * share, share), share)
    hidden = ALPHA * tokens[:, share_cols].astype(F32)

    @pl.loop(1, tp)
    def _(d):
        b_in(lax.rem(t + d, tp)).wait_recv()

    for p in range(tp):
        hidden = hidden + b_recv[p].astype(F32)

    rows[t, e] = hidden.astype(rows.dtype)

    def c_out(d):
        peer, pe, pt = other(d)
        return remote(rows.at[t, e], rows.at[t, e], c_ss.at[peer], c_rs.at[me], pe, pt)

    def c_in(d):
        peer, pe, pt = other(d)
        return remote(rows.at[t, e], rows.at[pt, pe], c_ss.at[peer], c_rs.at[peer], pe, pt)

    @pl.loop(1, n)
    def _(d):
        c_out(d).start()

    @pl.loop(1, n)
    def _(d):
        c_in(d).wait_recv()

    total = jnp.zeros((ep * seqs, 1), F32)
    for p in range(tp):
        block = rows[p].reshape(ep * seqs, share).astype(F32)
        total = total + jnp.sum(block, axis=1, keepdims=True)
    mean = total / width
    square = jnp.zeros((ep * seqs, 1), F32)
    for p in range(tp):
        block = rows[p].reshape(ep * seqs, share).astype(F32) - mean
        square = square + jnp.sum(block * block, axis=1, keepdims=True)
    scale = lax.rsqrt(square / width + EPSILON)
    for i in (1, 2):
        loads[i].wait()
    glu = jnp.zeros((ep * seqs, wg_v.shape[1]), F32)
    linear = jnp.zeros((ep * seqs, wg_v.shape[1]), F32)
    for p in range(tp):
        block = rows[p].reshape(ep * seqs, share).astype(F32)
        block = ((block - mean) * scale * gain[:, p * share : (p + 1) * share]).astype(BF16)
        normed[p] = block.reshape(ep, seqs, share)
        glu = glu + mm(block, wg_v[p * share : (p + 1) * share, :])
        linear = linear + mm(block, wl_v[p * share : (p + 1) * share, :])
    glu = jnp.minimum(glu, LIMIT)
    linear = jnp.clip(linear, -LIMIT, LIMIT)
    act = (glu * jax.nn.sigmoid(SLOPE * glu) * (linear + 1.0)).astype(BF16)
    loads[4].wait()

    for p in range(tp):
        part = mm(act, wd_v[:, p * share : (p + 1) * share]).astype(BF16)
        d_send[p] = part.reshape(ep, seqs, share)

    def d_out(d):
        peer, pe, pt = other(d)
        return remote(d_send.at[pt, pe], d_recv.at[e, t], d_ss.at[peer], d_rs.at[me], pe, pt)

    def d_in(d):
        peer, pe, pt = other(d)
        return remote(d_send.at[pt, pe], d_recv.at[pe, pt], d_ss.at[peer], d_rs.at[peer], pe, pt)

    @pl.loop(1, n)
    def _(d):
        d_out(d).start()

    d_recv[e, t] = d_send[t, e]
    loads[3].wait()
    logits = jnp.zeros((seqs, experts), F32)
    for p in range(tp):
        logits = logits + mm(normed[p, e], router_v[p * share : (p + 1) * share, :])
    ids = lax.broadcasted_iota(jnp.int32, (seqs, experts), 1)
    routed = ids == routing[:, 0:1]
    for j in range(1, routing.shape[1]):
        routed = routed | (ids == routing[:, j : j + 1])
    top = jnp.max(jnp.where(routed, logits, -jnp.inf), axis=1, keepdims=True)
    raised = jnp.where(routed, jnp.exp(jnp.where(routed, logits - top, 0.0)), 0.0)
    gates = raised / jnp.sum(raised, axis=1, keepdims=True)
    combined = ALPHA * normed[t, e].astype(F32)

    @pl.loop(1, n)
    def _(d):
        d_in(d).wait_recv()

    for x in range(ep):
        summed = d_recv[x, 0].astype(F32)
        for p in range(1, tp):
            summed = summed + d_recv[x, p].astype(F32)
        combined = combined + (summed * gates[:, x : x + 1]).astype(BF16).astype(F32)

    own_sum = jnp.sum(combined, axis=1, keepdims=True)
    centred = combined - own_sum / share
    own_square = jnp.sum(centred * centred, axis=1, keepdims=True)
    lane = lax.broadcasted_iota(jnp.int32, stats.shape[1:], 1)
    stats[t] = jnp.where(lane == 0, own_sum, own_square)

    def e_out(p):
        return remote(stats.at[t], stats.at[t], e_ss.at[p], e_rs.at[t], e, p)

    def e_in(p):
        return remote(stats.at[t], stats.at[p], e_ss.at[p], e_rs.at[p], e, p)

    @pl.loop(1, tp)
    def _(d):
        e_out(lax.rem(t + d, tp)).start()

    @pl.loop(1, tp)
    def _(d):
        e_in(lax.rem(t + d, tp)).wait_recv()

    sums = [stats[p][:, 0:1] for p in range(tp)]
    mean = functools.reduce(jnp.add, sums) / width
    square = jnp.zeros((seqs, 1), F32)
    for p in range(tp):
        gap = sums[p] / share - mean
        square = square + stats[p][:, 1:2] + share * gap * gap
    scale = lax.rsqrt(square / width + EPSILON)
    out[...] = ((combined - mean) * scale * final_gain[:, share_cols]).astype(BF16)

    @pl.loop(1, tp)
    def _(d):
        b_out(lax.rem(t + d, tp)).wait_send()
        e_out(lax.rem(t + d, tp)).wait_send()

    @pl.loop(1, n)
    def _(d):
        c_out(d).wait_send()
        d_out(d).wait_send()


def per_device(
    tokens, query_weight, key_weight, value_weight, decay_down, decay_up, decay_bias, old_state,
    out_weight, norm_gain, router_weight, routing, glu_weight, linear_weight, down_weight,
    final_gain,
):
    tp = lax.axis_size("tp")
    ep = lax.axis_size("ep")
    n = ep * tp
    seqs, width = tokens.shape
    dk, dv = old_state.shape[1:]
    heads = query_weight.shape[1] // dk
    share = width // tp
    lanes = -(-3 * seqs // 128) * 128
    vmem = pl.BlockSpec(memory_space=pltpu.VMEM)
    hbm = pl.BlockSpec(memory_space=pl.ANY)
    dma = pltpu.SemaphoreType.DMA

    pack, values = pl.pallas_call(
        functools.partial(project_kernel, tp, heads, dk),
        out_shape=(
            jax.ShapeDtypeStruct((dk, lanes), F32),
            jax.ShapeDtypeStruct((seqs, dv), F32),
        ),
        in_specs=[vmem, hbm, hbm, hbm, hbm, vmem, vmem],
        out_specs=(vmem, vmem),
        scratch_shapes=[
            pltpu.VMEM(query_weight.shape, BF16),
            pltpu.VMEM(key_weight.shape, BF16),
            pltpu.VMEM(value_weight.shape, BF16),
            pltpu.VMEM(decay_down.shape, BF16),
            pltpu.VMEM((heads, 2 * seqs, dk), BF16),
            pltpu.VMEM((tp, 2 * seqs, dk), BF16),
            dma((4,)),
            dma((tp,)),
            dma((tp,)),
        ],
        compiler_params=pltpu.CompilerParams(
            collective_id=0, has_side_effects=True, vmem_limit_bytes=16 * MIB
        ),
        name="project",
    )(
        tokens, query_weight, key_weight, value_weight, decay_down, decay_up,
        decay_bias.reshape(1, -1),
    )

    new_state, mixed = pl.pallas_call(
        state_kernel,
        out_shape=(
            jax.ShapeDtypeStruct(old_state.shape, F32),
            jax.ShapeDtypeStruct((seqs, dv), BF16),
        ),
        in_specs=[vmem, vmem, hbm],
        out_specs=(hbm, vmem),
        scratch_shapes=[
            pltpu.VMEM(old_state.shape, F32),
            pltpu.VMEM(old_state.shape, F32),
            dma((seqs,)),
            dma((seqs,)),
        ],
        compiler_params=pltpu.CompilerParams(vmem_limit_bytes=24 * MIB),
        name="state",
    )(pack, values, old_state)

    layer_out = pl.pallas_call(
        functools.partial(expert_kernel, ep, tp),
        out_shape=jax.ShapeDtypeStruct((seqs, share), BF16),
        in_specs=[vmem] * 5 + [hbm] * 5,
        out_specs=vmem,
        scratch_shapes=[
            pltpu.VMEM(out_weight.shape, BF16),
            pltpu.VMEM(router_weight.shape, BF16),
            pltpu.VMEM(glu_weight.shape[1:], BF16),
            pltpu.VMEM(linear_weight.shape[1:], BF16),
            pltpu.VMEM(down_weight.shape[1:], BF16),
            pltpu.VMEM((tp, seqs, share), BF16),
            pltpu.VMEM((tp, seqs, share), BF16),
            pltpu.VMEM((tp, ep, seqs, share), BF16),
            pltpu.VMEM((tp, ep, seqs, share), BF16),
            pltpu.VMEM((tp, ep, seqs, share), BF16),
            pltpu.VMEM((ep, tp, seqs, share), BF16),
            pltpu.VMEM((tp, seqs, 128), F32),
            dma((5,)),
            dma((tp,)),
            dma((tp,)),
            dma((n,)),
            dma((n,)),
            dma((n,)),
            dma((n,)),
            dma((tp,)),
            dma((tp,)),
        ],
        compiler_params=pltpu.CompilerParams(
            collective_id=1, has_side_effects=True, vmem_limit_bytes=32 * MIB
        ),
        name="experts",
    )(
        tokens, mixed, norm_gain.reshape(1, -1), final_gain.reshape(1, -1), routing, out_weight,
        router_weight, glu_weight, linear_weight, down_weight,
    )
    return (layer_out, new_state)


def solution(mesh):
    return jax.shard_map(
        per_device,
        mesh=mesh,
        in_specs=(
            P("ep", None),
            P("tp", None),
            P("tp", None),
            P(None, "tp"),
            P(),
            P(),
            P(),
            P("ep", None, "tp"),
            P("tp", None),
            P(),
            P(),
            P("ep", None),
            P("ep", None, "tp"),
            P("ep", None, "tp"),
            P("ep", "tp", None),
            P(),
        ),
        out_specs=(P("ep", "tp"), P("ep", None, "tp")),
        check_vma=False,
    )
```

time: 189 us -> 73.2 us (0.39)
  blocking collectives: 82.4 us -> 0 us
  Pallas kernels: 0 us -> 58.2 us
  waiting for transfers between devices: 56.2 us -> 0 us
  matrix products: 16.6 us -> 0 us
  between operations: 14.2 us -> 0.76 us
  local copies, waits for them, and re-layouts: 4.41 us -> 13.9 us
  other arithmetic: 7.34 us -> 0 us
  starting transfers between devices: 7.03 us -> 0 us
    psum x3 -> x0, blocking collectives: 58.9 us -> none  [the longest x1 31.6 us: per_device(): query_sum, key_sum = lax.psum((query_part, key_part), 'tp')]
    pallas_call x0 -> x3, Pallas kernels: none -> 58.2 us  [the longest x1 44.9 us: per_device(): pl.pallas_call(functools.partial(expert_kernel, ep, tp), out_shape=jax.Sh...]
    reduce_scatter x2 -> x0, waiting for transfers between devices: 47.4 us -> none  [the longest x1 27.6 us: per_device(): lax.psum_scatter(out_terms, 'tp', scatter_dimension=1, tiled=True)]
    dot_general x13 -> x0, matrix products: 16.6 us -> none  [the longest x1 3.99 us: per_device(): jnp.dot(act, down_local, preferred_element_type=jnp.float32)]
    all_gather x1 -> x0, blocking collectives: 14.9 us -> none  [per_device(): piece = lax.all_gather(rows_in, 'tp', axis=2, tiled=True)]
    unnamed x15 -> x36, local copies, waits for them, and re-layouts: 1.7 us -> 13.9 us
    all_to_all x2 -> x0, waiting for transfers between devices: 8.72 us -> none  [the longest x1 4.63 us: per_device(): lax.all_to_all(slot_ids, 'ep', split_axis=0, concat_axis=0, tiled=True)]
    all_to_all x1 -> x0, blocking collectives: 8.53 us -> none  [per_device(): lax.all_to_all(send_rows, 'ep', split_axis=0, concat_axis=0, tiled=True)]
  transfers between devices with their start and end apart: 4 -> 0, of which waited for: 4 -> 0; matrix products, arithmetic and copies ran while one was open for 2% -> 0% of each run, Pallas kernels for 0% -> 0%
where the time goes in v1:
time: 73.2 us; the launch traced here: 72.8 us
  Pallas kernels  58.2 us (80%)
  local copies, waits for them, and re-layouts  13.9 us (19%)
  between operations  0.76 us (1%)
    pallas_call x1, Pallas kernels, per_device(): pl.pallas_call(functools.partial(expert_kernel, ep, tp), out_shape=jax.Sh...  44.9 us
    unnamed x36, local copies, waits for them, and re-layouts  13.9 us
    pallas_call x1, Pallas kernels, per_device(): pl.pallas_call(functools.partial(project_kernel, tp, heads, dk), out_shap...  9.04 us
    pallas_call x1, Pallas kernels, per_device(): pl.pallas_call(state_kernel, out_shape=(jax.ShapeDtypeStruct(old_state.sh...  4.21 us

profile of v1, /device:TPU:0, one launch (start us, length us, event | category | flops | bytes accessed | tf_op | source)
XLA Modules:
  0.0 72.8 jit_solution(8445935185148578910)
XLA Ops:
  0.6 1.4 %copy.18.dd = bf16[4096,16]{1,0:T(8,128)(2,1)S(1)} copy(bf16[4096,16]{0,1:T(8,128)(2,1)} %param.20) | data formatting | bytes 262144 | tf_op args[4]
  2.0 0.0 copy-start.1
  2.0 1.6 %copy-done.1 = bf16[4096,256]{1,0:T(8,128)(2,1)S(1)} copy-done((bf16[4096,256]{1,0:T(8,128)(2,1)S(1)}, bf16[4096,256]{1,0:T(8,128)(2,1)}, u32[]{:S(2)}) %copy-start.1) | copy-done | bytes 2097176
  3.6 0.0 copy-start.6
  3.6 1.2 %copy-done.6 = bf16[512,1024]{1,0:T(8,128)(2,1)S(1)} copy-done((bf16[512,1024]{1,0:T(8,128)(2,1)S(1)}, bf16[512,1024]{1,0:T(8,128)(2,1)}, u32[]{:S(2)}) %copy-start.6) | copy-done | bytes 1048600
  4.8 0.0 copy-start.7
  4.8 1.2 %copy-done.7 = bf16[512,1024]{1,0:T(8,128)(2,1)S(1)} copy-done((bf16[512,1024]{1,0:T(8,128)(2,1)S(1)}, bf16[512,1024]{1,0:T(8,128)(2,1)}, u32[]{:S(2)}) %copy-start.7) | copy-done | bytes 1048600
  6.1 0.0 copy-start.8
  6.1 0.9 %copy-done.8 = bf16[16,4096]{1,0:T(8,128)(2,1)S(1)} copy-done((bf16[16,4096]{1,0:T(8,128)(2,1)S(1)}, bf16[16,4096]{1,0:T(8,128)(2,1)}, u32[]{:S(2)}) %copy-start.8) | copy-done | bytes 131096
  7.0 0.0 copy-start.10
  7.0 0.8 %copy-done.10 = f32[16,1024]{1,0:T(8,128)S(1)} copy-done((f32[16,1024]{1,0:T(8,128)S(1)}, f32[16,1024]{1,0:T(8,128)}, u32[]{:S(2)}) %copy-start.10) | copy-done | bytes 65560
  7.8 0.0 copy-start.13
  7.8 0.7 copy-done.13
  8.5 0.0 copy-start
  8.5 9.0 %project.1 = (f32[256,128]{1,0:T(8,128)S(1)}, f32[16,256]{1,0:T(8,128)S(1)}) custom-call(bf16[16,4096]{1,0:T(8,128)(2,1)S(1)} %copy-done.8, bf16[512,1024]{1,0:T(8,128)(2,1)S(1)} %copy-done.6, bf16[512,1024]{1,0:T(8,128)(2,1)S(1)} %copy-done.7, bf16[4096,256]{1,0:T(8,128)(2,1)S(1)} %copy-done.1, bf16[4096,16]{1,0:T(8,128)(2,1)S(1)} %copy.18.dd, ...), custom_call_target="tpu_custom_call" | custom-call | tf_op jit(solution)/shard_map/project/pallas_call | solution.py:335
  17.5 0.0 copy-done
  17.6 0.0 copy-start.14
  17.6 0.0 copy-start.15
  17.6 0.0 copy-start.2
  17.6 0.0 copy-start.9
  17.6 0.0 copy-start.11
  17.6 0.0 copy-start.12
  17.6 4.2 %state.1 = (f32[16,256,256]{2,1,0:T(8,128)}, bf16[16,256]{1,0:T(8,128)(2,1)S(1)}) custom-call(f32[256,128]{1,0:T(8,128)S(1)} %get-tuple-element.6.pack, f32[16,256]{1,0:T(8,128)S(1)} %get-tuple-element.7.values, f32[16,256,256]{2,1,0:T(8,128)S(1)} %copy-done), custom_call_target="tpu_custom_call" | custom-call | tf_op jit(solution)/shard_map/state/pallas_call | solution.py:363
  21.8 0.0 copy-done.14
  21.9 0.5 copy.20.router
  22.4 0.0 copy-done.15
  22.4 0.1 copy.19.routing
  22.5 0.0 copy-done.2
  22.5 0.0 copy-done.9
  22.5 0.0 copy-done.11
  22.5 0.0 copy-done.12
  22.5 0.0 copy-start.3
  22.5 1.6 %copy-done.3 = bf16[1,4096,256]{2,1,0:T(8,128)(2,1)S(1)} copy-done((bf16[1,4096,256]{2,1,0:T(8,128)(2,1)S(1)}, bf16[1,4096,256]{2,1,0:T(8,128)(2,1)}, u32[]{:S(2)}) %copy-start.3) | copy-done | bytes 2097176
  24.1 0.0 copy-start.4
  24.1 1.6 %copy-done.4 = bf16[1,4096,256]{2,1,0:T(8,128)(2,1)S(1)} copy-done((bf16[1,4096,256]{2,1,0:T(8,128)(2,1)S(1)}, bf16[1,4096,256]{2,1,0:T(8,128)(2,1)}, u32[]{:S(2)}) %copy-start.4) | copy-done | bytes 2097176
  25.7 0.0 copy-start.5
  25.7 1.6 %copy-done.5 = bf16[1,256,4096]{2,1,0:T(8,128)(2,1)S(1)} copy-done((bf16[1,256,4096]{2,1,0:T(8,128)(2,1)S(1)}, bf16[1,256,4096]{2,1,0:T(8,128)(2,1)}, u32[]{:S(2)}) %copy-start.5) | copy-done | bytes 2097176
  27.3 44.9 %experts.1 = bf16[16,512]{1,0:T(8,128)(2,1)S(1)} custom-call(bf16[16,4096]{1,0:T(8,128)(2,1)S(1)} %copy-done.9, bf16[16,256]{1,0:T(8,128)(2,1)S(1)} %get-tuple-element.8.mixed, f32[1,4096]{1,0:T(1,128)S(1)} %bitcast.3, f32[1,4096]{1,0:T(1,128)S(1)} %bitcast.4, s32[16,2]{1,0:T(8,128)S(1)} %copy.19.routing, bf16[256,4096]{1,0:T(8,128)(2,1)S(1)} %copy-done.2, ...), custom_call_target="tpu_custom_call" | custom-call | tf_op jit(solution)/shard_map/experts/pallas_call | solution.py:381
  72.2 0.6 copy.22
Async XLA Ops:
  2.0 1.6 %copy-start.1 = (bf16[4096,256]{1,0:T(8,128)(2,1)S(1)}, bf16[4096,256]{1,0:T(8,128)(2,1)}, u32[]{:S(2)}) copy-start(bf16[4096,256]{1,0:T(8,128)(2,1)} %wv.1) | copy-start | bytes 6291460
  3.6 1.2 %copy-start.6 = (bf16[512,1024]{1,0:T(8,128)(2,1)S(1)}, bf16[512,1024]{1,0:T(8,128)(2,1)}, u32[]{:S(2)}) copy-start(bf16[512,1024]{1,0:T(8,128)(2,1)} %wq.1) | copy-start | bytes 3145732
  4.8 1.2 %copy-start.7 = (bf16[512,1024]{1,0:T(8,128)(2,1)S(1)}, bf16[512,1024]{1,0:T(8,128)(2,1)}, u32[]{:S(2)}) copy-start(bf16[512,1024]{1,0:T(8,128)(2,1)} %wk.1) | copy-start | bytes 3145732
  6.1 0.9 %copy-start.8 = (bf16[16,4096]{1,0:T(8,128)(2,1)S(1)}, bf16[16,4096]{1,0:T(8,128)(2,1)}, u32[]{:S(2)}) copy-start(bf16[16,4096]{1,0:T(8,128)(2,1)} %tokens.3) | copy-start | bytes 393220
  7.0 0.8 %copy-start.10 = (f32[16,1024]{1,0:T(8,128)S(1)}, f32[16,1024]{1,0:T(8,128)}, u32[]{:S(2)}) copy-start(f32[16,1024]{1,0:T(8,128)} %up.1) | copy-start | bytes 196612
  7.8 0.7 copy-start.13
  8.5 9.1 %copy-start = (f32[16,256,256]{2,1,0:T(8,128)S(1)}, f32[16,256,256]{2,1,0:T(8,128)}, u32[]{:S(2)}) copy-start(f32[16,256,256]{2,1,0:T(8,128)} %old.1) | copy-start | bytes 12582916
  17.6 4.3 %copy-start.14 = (bf16[4096,4]{0,1:T(4,128)(2,1)S(1)}, bf16[4096,4]{0,1:T(4,128)(2,1)}, u32[]{:S(2)}) copy-start(bf16[4096,4]{0,1:T(4,128)(2,1)} %param.26) | copy-start | bytes 98308
  17.6 4.8 %copy-start.15 = (s32[16,2]{0,1:T(2,128)S(1)}, s32[16,2]{0,1:T(2,128)}, u32[]{:S(2)}) copy-start(s32[16,2]{0,1:T(2,128)} %param.27) | copy-start | bytes 388
  17.6 4.9 %copy-start.2 = (bf16[256,4096]{1,0:T(8,128)(2,1)S(1)}, bf16[256,4096]{1,0:T(8,128)(2,1)}, u32[]{:S(2)}) copy-start(bf16[256,4096]{1,0:T(8,128)(2,1)} %wo.1) | copy-start | bytes 6291460
  17.6 4.9 %copy-start.9 = (bf16[16,4096]{1,0:T(8,128)(2,1)S(1)}, bf16[16,4096]{1,0:T(8,128)(2,1)}, u32[]{:S(2)}) copy-start(bf16[16,4096]{1,0:T(8,128)(2,1)} %tokens.3) | copy-start | bytes 393220
  17.6 4.9 %copy-start.11 = (f32[4096]{0:T(1024)S(1)}, f32[4096]{0:T(1024)}, u32[]{:S(2)}) copy-start(f32[4096]{0:T(1024)} %param.25) | copy-start | bytes 49156
  17.6 4.9 %copy-start.12 = (f32[4096]{0:T(1024)S(1)}, f32[4096]{0:T(1024)}, u32[]{:S(2)}) copy-start(f32[4096]{0:T(1024)} %param.31) | copy-start | bytes 49156
  22.5 1.6 %copy-start.3 = (bf16[1,4096,256]{2,1,0:T(8,128)(2,1)S(1)}, bf16[1,4096,256]{2,1,0:T(8,128)(2,1)}, u32[]{:S(2)}) copy-start(bf16[1,4096,256]{2,1,0:T(8,128)(2,1)} %wg.1) | copy-start | bytes 6291460
  24.1 1.6 %copy-start.4 = (bf16[1,4096,256]{2,1,0:T(8,128)(2,1)S(1)}, bf16[1,4096,256]{2,1,0:T(8,128)(2,1)}, u32[]{:S(2)}) copy-start(bf16[1,4096,256]{2,1,0:T(8,128)(2,1)} %wl.1) | copy-start | bytes 6291460
  25.7 1.6 %copy-start.5 = (bf16[1,256,4096]{2,1,0:T(8,128)(2,1)S(1)}, bf16[1,256,4096]{2,1,0:T(8,128)(2,1)}, u32[]{:S(2)}) copy-start(bf16[1,256,4096]{2,1,0:T(8,128)(2,1)} %wd.1) | copy-start | bytes 6291460

commit v2 on v1

v2 whole, which is shorter than its diff:
```python
import functools

import jax
import jax.numpy as jnp
from jax import lax
from jax.experimental import pallas as pl
from jax.experimental.pallas import tpu as pltpu
from jax.sharding import PartitionSpec as P

ALPHA = 2.0**0.25
TAU = 16.0
LIMIT = 7.0
SLOPE = 1.702
EPSILON = 1e-05
MESH = pl.DeviceIdType.MESH
F32 = jnp.float32
BF16 = jnp.bfloat16
MIB = 1 << 20


def mm(a, b):
    return jnp.dot(a, b, preferred_element_type=F32)


def log_sigmoid(z):
    return jnp.minimum(z, 0.0) - jnp.log1p(jnp.exp(-jnp.abs(z)))


def project_kernel(
    tp, heads, dk, tokens_h, wq, wk, wv, dd, up_h, bias_h, pack_out, values_out,
    tokens, wq_v, wk_v, wv_v, dd_v, up, bias, send, recv, load_sem, send_sem, recv_sem,
):
    me = lax.axis_index("tp")
    pairs = (
        (tokens_h, tokens), (wq, wq_v), (wk, wk_v), (dd, dd_v), (up_h, up), (bias_h, bias),
        (wv, wv_v),
    )
    loads = [
        pltpu.make_async_copy(src, dst, load_sem.at[i]) for i, (src, dst) in enumerate(pairs)
    ]
    for load in loads:
        load.start()
    seqs, width = tokens.shape
    share = width // tp
    group = tp // heads
    barrier = pltpu.get_barrier_semaphore()

    @pl.loop(1, tp)
    def _(d):
        pl.semaphore_signal(
            barrier, inc=1, device_id={"tp": lax.rem(me + d, tp)}, device_id_type=MESH
        )

    loads[0].wait()
    own = tokens[:, pl.ds(pl.multiple_of(me * share, share), share)]
    for i, w in ((0, wq_v), (1, wk_v)):
        loads[1 + i].wait()
        part = mm(own, w[...])
        for h in range(heads):
            send[h, i * seqs : (i + 1) * seqs, :] = part[:, h * dk : (h + 1) * dk].astype(BF16)
    pl.semaphore_wait(barrier, tp - 1)

    def copy_to(peer):
        return pltpu.make_async_remote_copy(
            src_ref=send.at[peer // group],
            dst_ref=recv.at[me],
            send_sem=send_sem.at[peer],
            recv_sem=recv_sem.at[me],
            device_id={"tp": peer},
            device_id_type=MESH,
        )

    def copy_from(peer):
        return pltpu.make_async_remote_copy(
            src_ref=send.at[0],
            dst_ref=recv.at[peer],
            send_sem=send_sem.at[peer],
            recv_sem=recv_sem.at[peer],
            device_id={"tp": peer},
            device_id_type=MESH,
        )

    @pl.loop(1, tp)
    def _(d):
        copy_to(lax.rem(me + d, tp)).start()

    head = me // group
    recv[me] = send[head]
    loads[3].wait()
    low = lax.dot_general(
        tokens[...], dd_v[...], (((1,), (1,)), ((), ())), preferred_element_type=F32
    )
    loads[4].wait()
    loads[5].wait()
    cols = pl.ds(pl.multiple_of(head * dk, dk), dk)
    up_cols = up[:, cols]
    z = jnp.broadcast_to(bias[:, cols], (seqs, dk))
    for r in range(low.shape[1]):
        z = z + low[:, r : r + 1] * up_cols[r : r + 1, :]
    decay = jnp.exp(log_sigmoid(z) / TAU)
    loads[6].wait()
    values_out[...] = mm(tokens[...], wv_v[...]).astype(BF16).astype(F32)

    @pl.loop(1, tp)
    def _(d):
        copy_from(lax.rem(me + d, tp)).wait_recv()

    total = recv[0].astype(F32)
    for p in range(1, tp):
        total = total + recv[p].astype(F32)
    total = total.astype(BF16).astype(F32)
    pad = pack_out.shape[1] - 3 * seqs
    pack = jnp.concatenate([decay, total, jnp.zeros((pad, dk), F32)], axis=0)
    pack_out[...] = jnp.transpose(pack)

    @pl.loop(1, tp)
    def _(d):
        copy_to(lax.rem(me + d, tp)).wait_send()


def state_kernel(pack, values, old, new, mixed, new_v, out_sem):
    seqs, dk, dv = old.shape
    outs = [pltpu.make_async_copy(new_v.at[s], new.at[s], out_sem.at[s]) for s in range(seqs)]
    rows = []
    for s in range(seqs):
        value = values[s : s + 1, :]
        updated = pack[:, s : s + 1] * old[s] + pack[:, 2 * seqs + s : 2 * seqs + s + 1] * value
        new_v[s] = updated
        outs[s].start()
        rows.append(jnp.sum(pack[:, seqs + s : seqs + s + 1] * updated, axis=0, keepdims=True))
    mixed[...] = (jnp.concatenate(rows, axis=0) * dk ** (-0.5)).astype(BF16)
    for s in range(seqs):
        outs[s].wait()


def expert_kernel(
    ep, tp, tokens, mixed, gain, final_gain, routing, router, wo, wg, wl, wd, out,
    wg_v, wl_v, wd_v, b_send, b_recv, rows, normed, own_part, pair_send, pair_recv,
    d_send, d_recv, f_send, f_recv, stats,
    load_sem, b_ss, b_rs, z_ss, x_ss, p_ss, c_rs, dp_ss, dp_rs, d_ss, d_rs, f_ss, f_rs, e_ss, e_rs,
):
    e = lax.axis_index("ep")
    t = lax.axis_index("tp")
    n = ep * tp
    me = e * tp + t
    zs = tp // 2
    zi = t // 2
    c = lax.rem(t, 2)
    mate = t + 1 - 2 * c
    seqs, width = tokens.shape
    share = width // tp
    loads = [
        pltpu.make_async_copy(src, dst, load_sem.at[i])
        for i, (src, dst) in enumerate(((wg.at[0], wg_v), (wl.at[0], wl_v), (wd.at[0], wd_v)))
    ]
    for load in loads:
        load.start()
    barrier = pltpu.get_barrier_semaphore()

    @pl.loop(1, n)
    def _(d):
        peer = lax.rem(me + d, n)
        pl.semaphore_signal(
            barrier, inc=1, device_id={"ep": peer // tp, "tp": lax.rem(peer, tp)},
            device_id_type=MESH,
        )

    def remote(src, dst, ss, rs, pe, pt):
        return pltpu.make_async_remote_copy(
            src_ref=src, dst_ref=dst, send_sem=ss, recv_sem=rs,
            device_id={"ep": pe, "tp": pt}, device_id_type=MESH,
        )

    for p in range(tp):
        b_send[p] = mm(mixed[...], wo[:, p * share : (p + 1) * share]).astype(BF16)
    pl.semaphore_wait(barrier, n - 1)

    def b_out(p):
        return remote(b_send.at[p], b_recv.at[t], b_ss.at[p], b_rs.at[t], e, p)

    def b_in(p):
        return remote(b_send.at[p], b_recv.at[p], b_ss.at[p], b_rs.at[p], e, p)

    @pl.loop(1, tp)
    def _(d):
        b_out(lax.rem(t + d, tp)).start()

    b_recv[t] = b_send[t]
    share_cols = pl.ds(pl.multiple_of(t * share, share), share)
    hidden = ALPHA * tokens[:, share_cols].astype(F32)

    @pl.loop(1, tp)
    def _(d):
        b_in(lax.rem(t + d, tp)).wait_recv()

    for p in range(tp):
        hidden = hidden + b_recv[p].astype(F32)

    rows[t, e] = hidden.astype(rows.dtype)

    def block(z, core, x):
        return rows.at[2 * z + core, x], c_rs.at[2 * z + core, x]

    def z_out(z):
        ref, sem = block(zi, c, e)
        return remote(ref, ref, z_ss.at[z], sem, e, 2 * z + c)

    def z_in(z):
        ref, sem = block(z, c, e)
        return remote(ref, ref, z_ss.at[z], sem, e, 2 * z + c)

    def x_out(z, x):
        ref, sem = block(z, c, e)
        return remote(ref, ref, x_ss.at[z, x], sem, x, t)

    def x_in(z, x):
        ref, sem = block(z, c, x)
        return remote(ref, ref, x_ss.at[z, x], sem, x, t)

    def p_out(z, x):
        ref, sem = block(z, c, x)
        return remote(ref, ref, p_ss.at[z, x], sem, e, mate)

    def p_in(z, x):
        ref, sem = block(z, 1 - c, x)
        return remote(ref, ref, p_ss.at[z, x], sem, e, mate)

    def around(i, d, size):
        return lax.rem(i + d, size)

    @pl.loop(1, zs)
    def _(d):
        z_out(around(zi, d, zs)).start()

    @pl.loop(0, zs)
    def _(d):
        z = around(zi, d, zs)

        @pl.when(d > 0)
        def _():
            z_in(z).wait_recv()

        @pl.loop(1, ep)
        def _(k):
            x_out(z, around(e, k, ep)).start()

        p_out(z, e).start()

    @pl.loop(0, zs)
    def _(d):
        z = around(zi, d, zs)

        @pl.loop(1, ep)
        def _(k):
            x = around(e, k, ep)
            x_in(z, x).wait_recv()
            p_out(z, x).start()

    @pl.loop(0, zs)
    def _(d):
        z = around(zi, d, zs)

        @pl.loop(0, ep)
        def _(k):
            p_in(z, around(e, k, ep)).wait_recv()

    total = jnp.zeros((ep * seqs, 1), F32)
    for p in range(tp):
        part = rows[p].reshape(ep * seqs, share).astype(F32)
        total = total + jnp.sum(part, axis=1, keepdims=True)
    mean = total / width
    square = jnp.zeros((ep * seqs, 1), F32)
    for p in range(tp):
        part = rows[p].reshape(ep * seqs, share).astype(F32) - mean
        square = square + jnp.sum(part * part, axis=1, keepdims=True)
    scale = lax.rsqrt(square / width + EPSILON)
    for i in (0, 1):
        loads[i].wait()
    glu = jnp.zeros((ep * seqs, wg_v.shape[1]), F32)
    linear = jnp.zeros((ep * seqs, wg_v.shape[1]), F32)
    for p in range(tp):
        part = rows[p].reshape(ep * seqs, share).astype(F32)
        part = ((part - mean) * scale * gain[:, p * share : (p + 1) * share]).astype(BF16)
        normed[p] = part.reshape(ep, seqs, share)
        glu = glu + mm(part, wg_v[p * share : (p + 1) * share, :])
        linear = linear + mm(part, wl_v[p * share : (p + 1) * share, :])
    glu = jnp.minimum(glu, LIMIT)
    linear = jnp.clip(linear, -LIMIT, LIMIT)
    act = (glu * jax.nn.sigmoid(SLOPE * glu) * (linear + 1.0)).astype(BF16)
    loads[2].wait()

    def down(z, core):
        first = pl.multiple_of((2 * z + core) * share, share)
        return mm(act, wd_v[:, pl.ds(first, share)])

    def pair_copy(z):
        return remote(pair_send.at[z], pair_recv.at[z], dp_ss.at[z], dp_rs.at[z], e, mate)

    def d_out(z, x):
        return remote(d_send.at[z, x], d_recv.at[z, e], d_ss.at[z, x], d_rs.at[z, e], x, t)

    def d_in(z, x):
        return remote(d_send.at[z, x], d_recv.at[z, x], d_ss.at[z, x], d_rs.at[z, x], x, t)

    def f_out(z):
        return remote(f_send.at[z], f_recv.at[zi], f_ss.at[z], f_rs.at[zi], e, 2 * z + c)

    def f_in(z):
        return remote(f_send.at[z], f_recv.at[z], f_ss.at[z], f_rs.at[z], e, 2 * z + c)

    for d in range(1, zs + 1):
        z = around(zi, d, zs)
        pair_send[z] = down(z, 1 - c).astype(BF16)
        pair_copy(z).start()
    for d in range(1, zs + 1):
        z = around(zi, d, zs)
        own_part[z] = down(z, c)

    @pl.loop(1, zs + 1)
    def _(d):
        z = around(zi, d, zs)
        pair_copy(z).wait_recv()
        both = (own_part[z] + pair_recv[z].astype(F32)).astype(BF16)
        d_send[z] = both.reshape(ep, seqs, share)

        @pl.loop(1, ep)
        def _(k):
            d_out(z, around(e, k, ep)).start()

        d_recv[z, e] = d_send[z, e]

    experts = router.shape[0]
    logits = jnp.zeros((experts, seqs), F32)
    for p in range(tp):
        logits = logits + lax.dot_general(
            router[:, p * share : (p + 1) * share], normed[p, e], (((1,), (1,)), ((), ())),
            preferred_element_type=F32,
        )
    ids = lax.broadcasted_iota(jnp.int32, (experts, seqs), 0)
    routed = ids == routing[0:1, :]
    for j in range(1, routing.shape[0]):
        routed = routed | (ids == routing[j : j + 1, :])
    top = jnp.max(jnp.where(routed, logits, -jnp.inf), axis=0, keepdims=True)
    raised = jnp.where(routed, jnp.exp(jnp.where(routed, logits - top, 0.0)), 0.0)
    gates = raised / jnp.sum(raised, axis=0, keepdims=True)
    tall, wide = -(-experts // 8) * 8, 128
    gates = jnp.concatenate([gates, jnp.zeros((experts, wide - seqs), F32)], axis=1)
    if tall > experts:
        gates = jnp.concatenate([gates, jnp.zeros((tall - experts, wide), F32)], axis=0)
    gates = jnp.transpose(gates)[:seqs, :]
    combined = ALPHA * normed[t, e].astype(F32)

    @pl.loop(1, zs + 1)
    def _(d):
        z = around(zi, d, zs)

        @pl.loop(1, ep)
        def _(k):
            d_in(z, around(e, k, ep)).wait_recv()

        summed = jnp.zeros((seqs, share), F32)
        for x in range(ep):
            summed = summed + d_recv[z, x].astype(F32) * gates[:, x : x + 1]
        f_send[z] = summed.astype(BF16)

        @pl.when(d < zs)
        def _():
            f_out(z).start()

    f_recv[zi] = f_send[zi]

    @pl.loop(1, zs)
    def _(d):
        f_in(around(zi, d, zs)).wait_recv()

    for z in range(zs):
        combined = combined + f_recv[z].astype(F32)

    own_sum = jnp.sum(combined, axis=1, keepdims=True)
    centred = combined - own_sum / share
    own_square = jnp.sum(centred * centred, axis=1, keepdims=True)
    lane = lax.broadcasted_iota(jnp.int32, stats.shape[1:], 1)
    stats[t] = jnp.where(lane == 0, own_sum, own_square)

    def e_out(p):
        return remote(stats.at[t], stats.at[t], e_ss.at[p], e_rs.at[t], e, p)

    def e_in(p):
        return remote(stats.at[t], stats.at[p], e_ss.at[p], e_rs.at[p], e, p)

    @pl.loop(1, tp)
    def _(d):
        e_out(lax.rem(t + d, tp)).start()

    @pl.loop(1, tp)
    def _(d):
        e_in(lax.rem(t + d, tp)).wait_recv()

    sums = [stats[p][:, 0:1] for p in range(tp)]
    mean = functools.reduce(jnp.add, sums) / width
    square = jnp.zeros((seqs, 1), F32)
    for p in range(tp):
        gap = sums[p] / share - mean
        square = square + stats[p][:, 1:2] + share * gap * gap
    scale = lax.rsqrt(square / width + EPSILON)
    out[...] = ((combined - mean) * scale * final_gain[:, share_cols]).astype(BF16)

    @pl.loop(1, tp)
    def _(d):
        b_out(lax.rem(t + d, tp)).wait_send()
        e_out(lax.rem(t + d, tp)).wait_send()

    @pl.loop(0, zs)
    def _(d):
        z = around(zi, d, zs)

        @pl.when(d > 0)
        def _():
            z_out(z).wait_send()
            f_out(z).wait_send()

        pair_copy(z).wait_send()

        @pl.loop(0, ep)
        def _(k):
            x = around(e, k, ep)
            p_out(z, x).wait_send()

            @pl.when(k > 0)
            def _():
                x_out(z, x).wait_send()
                d_out(z, x).wait_send()


def per_device(
    tokens, query_weight, key_weight, value_weight, decay_down, decay_up, decay_bias, old_state,
    out_weight, norm_gain, router_weight, routing, glu_weight, linear_weight, down_weight,
    final_gain,
):
    tp = lax.axis_size("tp")
    ep = lax.axis_size("ep")
    n = ep * tp
    seqs, width = tokens.shape
    dk, dv = old_state.shape[1:]
    heads = query_weight.shape[1] // dk
    share = width // tp
    lanes = -(-3 * seqs // 128) * 128
    vmem = pl.BlockSpec(memory_space=pltpu.VMEM)
    hbm = pl.BlockSpec(memory_space=pltpu.HBM)
    zs = tp // 2
    dma = pltpu.SemaphoreType.DMA

    pack, values = pl.pallas_call(
        functools.partial(project_kernel, tp, heads, dk),
        out_shape=(
            jax.ShapeDtypeStruct((dk, lanes), F32),
            jax.ShapeDtypeStruct((seqs, dv), F32),
        ),
        in_specs=[hbm] * 7,
        out_specs=(vmem, vmem),
        scratch_shapes=[
            pltpu.VMEM(tokens.shape, BF16),
            pltpu.VMEM(query_weight.shape, BF16),
            pltpu.VMEM(key_weight.shape, BF16),
            pltpu.VMEM(value_weight.shape, BF16),
            pltpu.VMEM(decay_down.shape[::-1], BF16),
            pltpu.VMEM(decay_up.shape, F32),
            pltpu.VMEM((1, decay_bias.shape[0]), F32),
            pltpu.VMEM((heads, 2 * seqs, dk), BF16),
            pltpu.VMEM((tp, 2 * seqs, dk), BF16),
            dma((7,)),
            dma((tp,)),
            dma((tp,)),
        ],
        compiler_params=pltpu.CompilerParams(
            collective_id=0, has_side_effects=True, vmem_limit_bytes=16 * MIB
        ),
        name="project",
    )(
        tokens, query_weight, key_weight, value_weight, decay_down.T, decay_up,
        decay_bias.reshape(1, -1),
    )

    new_state, mixed = pl.pallas_call(
        state_kernel,
        out_shape=(
            jax.ShapeDtypeStruct(old_state.shape, F32),
            jax.ShapeDtypeStruct((seqs, dv), BF16),
        ),
        in_specs=[vmem, vmem, vmem],
        out_specs=(hbm, vmem),
        scratch_shapes=[
            pltpu.VMEM(old_state.shape, F32),
            dma((seqs,)),
        ],
        compiler_params=pltpu.CompilerParams(vmem_limit_bytes=24 * MIB),
        name="state",
    )(pack, values, old_state)

    layer_out = pl.pallas_call(
        functools.partial(expert_kernel, ep, tp),
        out_shape=jax.ShapeDtypeStruct((seqs, share), BF16),
        in_specs=[vmem] * 7 + [hbm] * 3,
        out_specs=vmem,
        scratch_shapes=[
            pltpu.VMEM(glu_weight.shape[1:], BF16),
            pltpu.VMEM(linear_weight.shape[1:], BF16),
            pltpu.VMEM(down_weight.shape[1:], BF16),
            pltpu.VMEM((tp, seqs, share), BF16),
            pltpu.VMEM((tp, seqs, share), BF16),
            pltpu.VMEM((tp, ep, seqs, share), BF16),
            pltpu.VMEM((tp, ep, seqs, share), BF16),
            pltpu.VMEM((zs, ep * seqs, share), F32),
            pltpu.VMEM((zs, ep * seqs, share), BF16),
            pltpu.VMEM((zs, ep * seqs, share), BF16),
            pltpu.VMEM((zs, ep, seqs, share), BF16),
            pltpu.VMEM((zs, ep, seqs, share), BF16),
            pltpu.VMEM((zs, seqs, share), BF16),
            pltpu.VMEM((zs, seqs, share), BF16),
            pltpu.VMEM((tp, seqs, 128), F32),
            dma((3,)),
            dma((tp,)),
            dma((tp,)),
            dma((zs,)),
            dma((zs, ep)),
            dma((zs, ep)),
            dma((tp, ep)),
            dma((zs,)),
            dma((zs,)),
            dma((zs, ep)),
            dma((zs, ep)),
            dma((zs,)),
            dma((zs,)),
            dma((tp,)),
            dma((tp,)),
        ],
        compiler_params=pltpu.CompilerParams(
            collective_id=1, has_side_effects=True, vmem_limit_bytes=32 * MIB
        ),
        name="experts",
    )(
        tokens, mixed, norm_gain.reshape(1, -1), final_gain.reshape(1, -1), routing.T,
        router_weight.T, out_weight, glu_weight, linear_weight, down_weight,
    )
    return (layer_out, new_state)


def solution(mesh):
    return jax.shard_map(
        per_device,
        mesh=mesh,
        in_specs=(
            P("ep", None),
            P("tp", None),
            P("tp", None),
            P(None, "tp"),
            P(),
            P(),
            P(),
            P("ep", None, "tp"),
            P("tp", None),
            P(),
            P(),
            P("ep", None),
            P("ep", None, "tp"),
            P("ep", None, "tp"),
            P("ep", "tp", None),
            P(),
        ),
        out_specs=(P("ep", "tp"), P("ep", None, "tp")),
        check_vma=False,
    )
```

time: 73.2 us -> 60.4 us (0.83)
  Pallas kernels: 58.2 us -> 47.1 us
  local copies, waits for them, and re-layouts: 13.9 us -> 12.2 us
    pallas_call x1, Pallas kernels: 44.9 us -> 34.9 us  [per_device(): pl.pallas_call(functools.partial(expert_kernel, ep, tp), out_shape=jax.Sh...]
    unnamed x36 -> x35, local copies, waits for them, and re-layouts: 13.9 us -> 12.2 us
    pallas_call x1, Pallas kernels: 4.21 us -> 2.6 us  [per_device(): pl.pallas_call(state_kernel, out_shape=(jax.ShapeDtypeStruct(old_state.sh...]
where the time goes in v2:
time: 60.4 us; the launch traced here: 60 us
  Pallas kernels  47.1 us (78%)
  local copies, waits for them, and re-layouts  12.2 us (20%)
  between operations  0.75 us (1%)
    pallas_call x1, Pallas kernels, per_device(): pl.pallas_call(functools.partial(expert_kernel, ep, tp), out_shape=jax.Sh...  34.9 us
    unnamed x35, local copies, waits for them, and re-layouts  12.2 us
    pallas_call x1, Pallas kernels, per_device(): pl.pallas_call(functools.partial(project_kernel, tp, heads, dk), out_shap...  9.51 us
    pallas_call x1, Pallas kernels, per_device(): pl.pallas_call(state_kernel, out_shape=(jax.ShapeDtypeStruct(old_state.sh...  2.6 us

profile of v2, /device:TPU:0, one launch (start us, length us, event | category | flops | bytes accessed | tf_op | source)
XLA Modules:
  0.0 60.0 jit_solution(4488985425201516986)
XLA Ops:
  0.6 0.0 copy-start.1
  0.6 1.6 %copy-done.1 = bf16[4096,256]{1,0:T(8,128)(2,1)S(1)} copy-done((bf16[4096,256]{1,0:T(8,128)(2,1)S(1)}, bf16[4096,256]{1,0:T(8,128)(2,1)}, u32[]{:S(2)}) %copy-start.1) | copy-done | bytes 2097176
  2.2 0.0 copy-start.6
  2.2 1.2 %copy-done.6 = bf16[512,1024]{1,0:T(8,128)(2,1)S(1)} copy-done((bf16[512,1024]{1,0:T(8,128)(2,1)S(1)}, bf16[512,1024]{1,0:T(8,128)(2,1)}, u32[]{:S(2)}) %copy-start.6) | copy-done | bytes 1048600
  3.5 0.0 copy-start.7
  3.5 1.2 %copy-done.7 = bf16[512,1024]{1,0:T(8,128)(2,1)S(1)} copy-done((bf16[512,1024]{1,0:T(8,128)(2,1)S(1)}, bf16[512,1024]{1,0:T(8,128)(2,1)}, u32[]{:S(2)}) %copy-start.7) | copy-done | bytes 1048600
  4.7 0.0 copy-start.8
  4.7 0.9 %copy-done.8 = bf16[16,4096]{1,0:T(8,128)(2,1)S(1)} copy-done((bf16[16,4096]{1,0:T(8,128)(2,1)S(1)}, bf16[16,4096]{1,0:T(8,128)(2,1)}, u32[]{:S(2)}) %copy-start.8) | copy-done | bytes 131096
  5.6 0.0 copy-start.10
  5.6 0.9 %copy-done.10 = bf16[4096,16]{0,1:T(8,128)(2,1)S(1)} copy-done((bf16[4096,16]{0,1:T(8,128)(2,1)S(1)}, bf16[4096,16]{0,1:T(8,128)(2,1)}, u32[]{:S(2)}) %copy-start.10) | copy-done | bytes 131096
  6.5 0.0 copy-start.11
  6.5 0.8 %copy-done.11 = f32[16,1024]{1,0:T(8,128)S(1)} copy-done((f32[16,1024]{1,0:T(8,128)S(1)}, f32[16,1024]{1,0:T(8,128)}, u32[]{:S(2)}) %copy-start.11) | copy-done | bytes 65560
  7.3 0.0 copy-start.15
  7.3 0.7 %copy-done.15 = f32[1024]{0:T(1024)S(1)} copy-done((f32[1024]{0:T(1024)S(1)}, f32[1024]{0:T(1024)}, u32[]{:S(2)}) %copy-start.15) | copy-done | bytes 4120
  8.0 0.0 copy-start
  8.0 0.0 copy-start.12
  8.0 0.0 copy-start.14
  8.0 9.5 %project.1 = (f32[256,128]{1,0:T(8,128)S(1)}, f32[16,256]{1,0:T(8,128)S(1)}) custom-call(bf16[16,4096]{1,0:T(8,128)(2,1)S(1)} %copy-done.8, bf16[512,1024]{1,0:T(8,128)(2,1)S(1)} %copy-done.6, bf16[512,1024]{1,0:T(8,128)(2,1)S(1)} %copy-done.7, bf16[4096,256]{1,0:T(8,128)(2,1)S(1)} %copy-done.1, bf16[16,4096]{1,0:T(8,128)(2,1)S(1)} %bitcast.6, ...), custom_call_target="tpu_custom_call" | custom-call | tf_op jit(solution)/shard_map/project/pallas_call | solution.py:453
  17.5 0.0 copy-done
  17.6 0.0 copy-start.2
  17.6 0.0 copy-start.3
  17.6 0.0 copy-start.9
  17.6 0.0 copy-start.13
  17.6 0.0 copy-start.16
  17.6 2.6 %state.1 = (f32[16,256,256]{2,1,0:T(8,128)}, bf16[16,256]{1,0:T(8,128)(2,1)S(1)}) custom-call(f32[256,128]{1,0:T(8,128)S(1)} %get-tuple-element.6.pack, f32[16,256]{1,0:T(8,128)S(1)} %get-tuple-element.7.values, f32[16,256,256]{2,1,0:T(8,128)S(1)} %copy-done), custom_call_target="tpu_custom_call" | custom-call | tf_op jit(solution)/shard_map/state/pallas_call | solution.py:484
  20.2 0.0 copy-done.12
  20.2 0.0 copy-done.14
  20.2 0.0 copy-done.2
  20.3 1.0 %copy-done.3 = bf16[1,4096,256]{2,1,0:T(8,128)(2,1)S(1)} copy-done((bf16[1,4096,256]{2,1,0:T(8,128)(2,1)S(1)}, bf16[1,4096,256]{2,1,0:T(8,128)(2,1)}, u32[]{:S(2)}) %copy-start.3) | copy-done | bytes 2097176
  21.3 0.0 copy-done.9
  21.3 0.0 copy-done.13
  21.3 0.0 copy-done.16
  21.3 0.0 copy-start.4
  21.3 1.6 %copy-done.4 = bf16[1,4096,256]{2,1,0:T(8,128)(2,1)S(1)} copy-done((bf16[1,4096,256]{2,1,0:T(8,128)(2,1)S(1)}, bf16[1,4096,256]{2,1,0:T(8,128)(2,1)}, u32[]{:S(2)}) %copy-start.4) | copy-done | bytes 2097176
  22.9 0.0 copy-start.5
  22.9 1.6 %copy-done.5 = bf16[1,256,4096]{2,1,0:T(8,128)(2,1)S(1)} copy-done((bf16[1,256,4096]{2,1,0:T(8,128)(2,1)S(1)}, bf16[1,256,4096]{2,1,0:T(8,128)(2,1)}, u32[]{:S(2)}) %copy-start.5) | copy-done | bytes 2097176
  24.5 34.9 %experts.1 = bf16[16,512]{1,0:T(8,128)(2,1)S(1)} custom-call(bf16[16,4096]{1,0:T(8,128)(2,1)S(1)} %copy-done.9, bf16[16,256]{1,0:T(8,128)(2,1)S(1)} %get-tuple-element.8.mixed, f32[1,4096]{1,0:T(1,128)S(1)} %bitcast.8, f32[1,4096]{1,0:T(1,128)S(1)} %bitcast.9, s32[2,16]{1,0:T(2,128)S(1)} %bitcast.11, bf16[4,4096]{1,0:T(4,128)(2,1)S(1)} %bitcast.7, ...), custom_call_target="tpu_custom_call" | custom-call | tf_op jit(solution)/shard_map/experts/pallas_call | solution.py:500
  59.4 0.6 %copy.19 = bf16[16,512]{1,0:T(8,128)(2,1)} copy(bf16[16,512]{1,0:T(8,128)(2,1)S(1)} %experts.1) | data formatting | bytes 32768
Async XLA Ops:
  0.6 1.6 %copy-start.1 = (bf16[4096,256]{1,0:T(8,128)(2,1)S(1)}, bf16[4096,256]{1,0:T(8,128)(2,1)}, u32[]{:S(2)}) copy-start(bf16[4096,256]{1,0:T(8,128)(2,1)} %wv.1) | copy-start | bytes 6291460
  2.2 1.2 %copy-start.6 = (bf16[512,1024]{1,0:T(8,128)(2,1)S(1)}, bf16[512,1024]{1,0:T(8,128)(2,1)}, u32[]{:S(2)}) copy-start(bf16[512,1024]{1,0:T(8,128)(2,1)} %wq.1) | copy-start | bytes 3145732
  3.5 1.2 %copy-start.7 = (bf16[512,1024]{1,0:T(8,128)(2,1)S(1)}, bf16[512,1024]{1,0:T(8,128)(2,1)}, u32[]{:S(2)}) copy-start(bf16[512,1024]{1,0:T(8,128)(2,1)} %wk.1) | copy-start | bytes 3145732
  4.7 0.9 %copy-start.8 = (bf16[16,4096]{1,0:T(8,128)(2,1)S(1)}, bf16[16,4096]{1,0:T(8,128)(2,1)}, u32[]{:S(2)}) copy-start(bf16[16,4096]{1,0:T(8,128)(2,1)} %tokens.1) | copy-start | bytes 393220
  5.6 0.9 %copy-start.10 = (bf16[4096,16]{0,1:T(8,128)(2,1)S(1)}, bf16[4096,16]{0,1:T(8,128)(2,1)}, u32[]{:S(2)}) copy-start(bf16[4096,16]{0,1:T(8,128)(2,1)} %param.20) | copy-start | bytes 393220
  6.5 0.8 %copy-start.11 = (f32[16,1024]{1,0:T(8,128)S(1)}, f32[16,1024]{1,0:T(8,128)}, u32[]{:S(2)}) copy-start(f32[16,1024]{1,0:T(8,128)} %up_h.1) | copy-start | bytes 196612
  7.3 0.7 %copy-start.15 = (f32[1024]{0:T(1024)S(1)}, f32[1024]{0:T(1024)}, u32[]{:S(2)}) copy-start(f32[1024]{0:T(1024)} %param.22) | copy-start | bytes 12292
  8.0 9.5 %copy-start = (f32[16,256,256]{2,1,0:T(8,128)S(1)}, f32[16,256,256]{2,1,0:T(8,128)}, u32[]{:S(2)}) copy-start(f32[16,256,256]{2,1,0:T(8,128)} %old.1) | copy-start | bytes 12582916
  8.0 12.2 %copy-start.12 = (bf16[4096,4]{0,1:T(4,128)(2,1)S(1)}, bf16[4096,4]{0,1:T(4,128)(2,1)}, u32[]{:S(2)}) copy-start(bf16[4096,4]{0,1:T(4,128)(2,1)} %param.26) | copy-start | bytes 98308
  8.0 12.2 %copy-start.14 = (f32[4096]{0:T(1024)S(1)}, f32[4096]{0:T(1024)}, u32[]{:S(2)}) copy-start(f32[4096]{0:T(1024)} %param.31) | copy-start | bytes 49156
  17.6 2.7 %copy-start.2 = (bf16[256,4096]{1,0:T(8,128)(2,1)S(1)}, bf16[256,4096]{1,0:T(8,128)(2,1)}, u32[]{:S(2)}) copy-start(bf16[256,4096]{1,0:T(8,128)(2,1)} %wo.1) | copy-start | bytes 6291460
  17.6 3.7 %copy-start.3 = (bf16[1,4096,256]{2,1,0:T(8,128)(2,1)S(1)}, bf16[1,4096,256]{2,1,0:T(8,128)(2,1)}, u32[]{:S(2)}) copy-start(bf16[1,4096,256]{2,1,0:T(8,128)(2,1)} %wg.1) | copy-start | bytes 6291460
  17.6 3.7 %copy-start.9 = (bf16[16,4096]{1,0:T(8,128)(2,1)S(1)}, bf16[16,4096]{1,0:T(8,128)(2,1)}, u32[]{:S(2)}) copy-start(bf16[16,4096]{1,0:T(8,128)(2,1)} %tokens.1) | copy-start | bytes 393220
  17.6 3.7 %copy-start.13 = (f32[4096]{0:T(1024)S(1)}, f32[4096]{0:T(1024)}, u32[]{:S(2)}) copy-start(f32[4096]{0:T(1024)} %param.25) | copy-start | bytes 49156
  17.6 3.7 %copy-start.16 = (s32[16,2]{0,1:T(2,128)S(1)}, s32[16,2]{0,1:T(2,128)}, u32[]{:S(2)}) copy-start(s32[16,2]{0,1:T(2,128)} %param.27) | copy-start | bytes 388
  21.3 1.6 %copy-start.4 = (bf16[1,4096,256]{2,1,0:T(8,128)(2,1)S(1)}, bf16[1,4096,256]{2,1,0:T(8,128)(2,1)}, u32[]{:S(2)}) copy-start(bf16[1,4096,256]{2,1,0:T(8,128)(2,1)} %wl.1) | copy-start | bytes 6291460
  22.9 1.6 %copy-start.5 = (bf16[1,256,4096]{2,1,0:T(8,128)(2,1)S(1)}, bf16[1,256,4096]{2,1,0:T(8,128)(2,1)}, u32[]{:S(2)}) copy-start(bf16[1,256,4096]{2,1,0:T(8,128)(2,1)} %wd.1) | copy-start | bytes 6291460

commit v3 on v2

--- a/solution.py
+++ b/solution.py
@@ -448,6 +448,7 @@
     vmem = pl.BlockSpec(memory_space=pltpu.VMEM)
     hbm = pl.BlockSpec(memory_space=pltpu.HBM)
     zs = tp // 2
+    keep = lambda x: pltpu.with_memory_space_constraint(x, pltpu.HBM)
     dma = pltpu.SemaphoreType.DMA
 
     pack, values = pl.pallas_call(
@@ -477,8 +478,8 @@
         ),
         name="project",
     )(
-        tokens, query_weight, key_weight, value_weight, decay_down.T, decay_up,
-        decay_bias.reshape(1, -1),
+        keep(tokens), keep(query_weight), keep(key_weight), keep(value_weight),
+        keep(decay_down.T), keep(decay_up), keep(decay_bias.reshape(1, -1)),
     )
 
     new_state, mixed = pl.pallas_call(
@@ -540,7 +541,7 @@
         name="experts",
     )(
         tokens, mixed, norm_gain.reshape(1, -1), final_gain.reshape(1, -1), routing.T,
-        router_weight.T, out_weight, glu_weight, linear_weight, down_weight,
+        router_weight.T, out_weight, keep(glu_weight), keep(linear_weight), keep(down_weight),
     )
     return (layer_out, new_state)
 

time: 60.4 us -> 47.6 us (0.79)
  local copies, waits for them, and re-layouts: 12.2 us -> 0.65 us
  Pallas kernels: 47.1 us -> 46 us
    unnamed x35 -> x15, local copies, waits for them, and re-layouts: 12.2 us -> 0.65 us
    pallas_call x1, Pallas kernels: 34.9 us -> 33.9 us  [per_device(): pl.pallas_call(functools.partial(expert_kernel, ep, tp), out_shape=jax.Sh...]
where the time goes in v3:
time: 47.6 us; the launch traced here: 47.4 us
  Pallas kernels  46 us (97%)
  between operations  0.77 us (2%)
  local copies, waits for them, and re-layouts  0.65 us (1%)
    pallas_call x1, Pallas kernels, per_device(): pl.pallas_call(functools.partial(expert_kernel, ep, tp), out_shape=jax.Sh...  33.9 us
    pallas_call x1, Pallas kernels, per_device(): pl.pallas_call(functools.partial(project_kernel, tp, heads, dk), out_shap...  9.54 us
    pallas_call x1, Pallas kernels, per_device(): pl.pallas_call(state_kernel, out_shape=(jax.ShapeDtypeStruct(old_state.sh...  2.6 us

profile of v3, /device:TPU:0, one launch (start us, length us, event | category | flops | bytes accessed | tf_op | source)
XLA Modules:
  0.0 47.4 jit_solution(644767076224489143)
XLA Ops:
  0.6 0.0 copy-start
  0.6 9.5 %project.1 = (f32[256,128]{1,0:T(8,128)S(1)}, f32[16,256]{1,0:T(8,128)S(1)}) custom-call(bf16[16,4096]{1,0:T(8,128)(2,1)} %tokens.1, bf16[512,1024]{1,0:T(8,128)(2,1)} %wq.1, bf16[512,1024]{1,0:T(8,128)(2,1)} %wk.1, bf16[4096,256]{1,0:T(8,128)(2,1)} %wv.1, bf16[16,4096]{1,0:T(8,128)(2,1)} %bitcast.10, f32[16,1024]{1,0:T(8,128)} %up_h.1, f32[1,1024]{1,0:T(1,128)} %bitcast.11), custom_call_target="tpu_custom_call" | custom-call | tf_op jit(solution)/shard_map/project/pallas_call | solution.py:454
  10.2 0.0 copy-done
  10.2 0.0 copy-start.1
  10.2 0.0 copy-start.2
  10.2 0.0 copy-start.3
  10.2 0.0 copy-start.4
  10.3 0.0 copy-start.5
  10.3 0.0 copy-start.6
  10.3 2.6 %state.1 = (f32[16,256,256]{2,1,0:T(8,128)}, bf16[16,256]{1,0:T(8,128)(2,1)S(1)}) custom-call(f32[256,128]{1,0:T(8,128)S(1)} %get-tuple-element.6.pack, f32[16,256]{1,0:T(8,128)S(1)} %get-tuple-element.7.values, f32[16,256,256]{2,1,0:T(8,128)S(1)} %copy-done), custom_call_target="tpu_custom_call" | custom-call | tf_op jit(solution)/shard_map/state/pallas_call | solution.py:485
  12.9 0.0 copy-done.1
  12.9 0.0 copy-done.2
  12.9 0.0 copy-done.3
  12.9 0.0 copy-done.4
  12.9 0.0 copy-done.5
  12.9 0.0 copy-done.6
  12.9 33.9 %experts.1 = bf16[16,512]{1,0:T(8,128)(2,1)S(1)} custom-call(bf16[16,4096]{1,0:T(8,128)(2,1)S(1)} %copy-done.2, bf16[16,256]{1,0:T(8,128)(2,1)S(1)} %get-tuple-element.8.mixed, f32[1,4096]{1,0:T(1,128)S(1)} %bitcast.7, f32[1,4096]{1,0:T(1,128)S(1)} %bitcast.8, s32[2,16]{1,0:T(2,128)S(1)} %bitcast.9, bf16[4,4096]{1,0:T(4,128)(2,1)S(1)} %bitcast.6, ...), custom_call_target="tpu_custom_call" | custom-call | tf_op jit(solution)/shard_map/experts/pallas_call | solution.py:501
  46.8 0.6 %copy.19 = bf16[16,512]{1,0:T(8,128)(2,1)} copy(bf16[16,512]{1,0:T(8,128)(2,1)S(1)} %experts.1) | data formatting | bytes 32768
Async XLA Ops:
  0.6 9.6 %copy-start = (f32[16,256,256]{2,1,0:T(8,128)S(1)}, f32[16,256,256]{2,1,0:T(8,128)}, u32[]{:S(2)}) copy-start(f32[16,256,256]{2,1,0:T(8,128)} %old.1) | copy-start | bytes 12582916
  10.2 2.7 %copy-start.1 = (bf16[256,4096]{1,0:T(8,128)(2,1)S(1)}, bf16[256,4096]{1,0:T(8,128)(2,1)}, u32[]{:S(2)}) copy-start(bf16[256,4096]{1,0:T(8,128)(2,1)} %wo.1) | copy-start | bytes 6291460
  10.2 2.7 %copy-start.2 = (bf16[16,4096]{1,0:T(8,128)(2,1)S(1)}, bf16[16,4096]{1,0:T(8,128)(2,1)}, u32[]{:S(2)}) copy-start(bf16[16,4096]{1,0:T(8,128)(2,1)} %tokens.1) | copy-start | bytes 393220
  10.2 2.7 %copy-start.3 = (bf16[4096,4]{0,1:T(4,128)(2,1)S(1)}, bf16[4096,4]{0,1:T(4,128)(2,1)}, u32[]{:S(2)}) copy-start(bf16[4096,4]{0,1:T(4,128)(2,1)} %param.26) | copy-start | bytes 98308
  10.2 2.7 %copy-start.4 = (f32[4096]{0:T(1024)S(1)}, f32[4096]{0:T(1024)}, u32[]{:S(2)}) copy-start(f32[4096]{0:T(1024)} %param.25) | copy-start | bytes 49156
  10.3 2.7 %copy-start.5 = (f32[4096]{0:T(1024)S(1)}, f32[4096]{0:T(1024)}, u32[]{:S(2)}) copy-start(f32[4096]{0:T(1024)} %param.31) | copy-start | bytes 49156
  10.3 2.7 %copy-start.6 = (s32[16,2]{0,1:T(2,128)S(1)}, s32[16,2]{0,1:T(2,128)}, u32[]{:S(2)}) copy-start(s32[16,2]{0,1:T(2,128)} %param.27) | copy-start | bytes 388

commit v4 on v3

--- a/solution.py
+++ b/solution.py
@@ -135,14 +135,12 @@
 
 def expert_kernel(
     ep, tp, tokens, mixed, gain, final_gain, routing, router, wo, wg, wl, wd, out,
-    wg_v, wl_v, wd_v, b_send, b_recv, rows, normed, own_part, pair_send, pair_recv,
+    wg_v, wl_v, wd_v, q_part, q_send, q_recv, b_send, b_recv, rows, normed, own_part, pair_send, pair_recv,
     d_send, d_recv, f_send, f_recv, stats,
-    load_sem, b_ss, b_rs, z_ss, x_ss, p_ss, c_rs, dp_ss, dp_rs, d_ss, d_rs, f_ss, f_rs, e_ss, e_rs,
+    load_sem, q_ss, q_rs, b_ss, b_rs, z_ss, x_ss, p_ss, c_rs, dp_ss, dp_rs, d_ss, d_rs, f_ss, f_rs, e_ss, e_rs,
 ):
     e = lax.axis_index("ep")
     t = lax.axis_index("tp")
-    n = ep * tp
-    me = e * tp + t
     zs = tp // 2
     zi = t // 2
     c = lax.rem(t, 2)
@@ -157,12 +155,16 @@
         load.start()
     barrier = pltpu.get_barrier_semaphore()
 
-    @pl.loop(1, n)
-    def _(d):
-        peer = lax.rem(me + d, n)
+    @pl.loop(1, tp)
+    def _(d):
         pl.semaphore_signal(
-            barrier, inc=1, device_id={"ep": peer // tp, "tp": lax.rem(peer, tp)},
-            device_id_type=MESH,
+            barrier, inc=1, device_id={"ep": e, "tp": lax.rem(t + d, tp)}, device_id_type=MESH
+        )
+
+    @pl.loop(1, ep)
+    def _(d):
+        pl.semaphore_signal(
+            barrier, inc=1, device_id={"ep": lax.rem(e + d, ep), "tp": t}, device_id_type=MESH
         )
 
     def remote(src, dst, ss, rs, pe, pt):
@@ -171,30 +173,57 @@
             device_id={"ep": pe, "tp": pt}, device_id_type=MESH,
         )
 
-    for p in range(tp):
-        b_send[p] = mm(mixed[...], wo[:, p * share : (p + 1) * share]).astype(BF16)
-    pl.semaphore_wait(barrier, n - 1)
-
-    def b_out(p):
-        return remote(b_send.at[p], b_recv.at[t], b_ss.at[p], b_rs.at[t], e, p)
-
-    def b_in(p):
-        return remote(b_send.at[p], b_recv.at[p], b_ss.at[p], b_rs.at[p], e, p)
-
-    @pl.loop(1, tp)
-    def _(d):
-        b_out(lax.rem(t + d, tp)).start()
-
-    b_recv[t] = b_send[t]
+    def around(i, d, size):
+        return lax.rem(i + d, size)
+
+    def project(z, core):
+        first = pl.multiple_of((2 * z + core) * share, share)
+        return mm(mixed[...], wo[:, pl.ds(first, share)])
+
+    def q_copy(z):
+        return remote(q_send.at[z], q_recv.at[z], q_ss.at[z], q_rs.at[z], e, mate)
+
+    def b_out(z):
+        return remote(b_send.at[z], b_recv.at[zi], b_ss.at[z], b_rs.at[zi], e, 2 * z + c)
+
+    def b_in(z):
+        return remote(b_send.at[z], b_recv.at[z], b_ss.at[z], b_rs.at[z], e, 2 * z + c)
+
+    for d in range(1, zs + 1):
+        z = around(zi, d, zs)
+        q_send[z] = project(z, 1 - c).astype(BF16)
+    pl.semaphore_wait(barrier, tp + ep - 2)
+
+    @pl.loop(1, zs + 1)
+    def _(d):
+        q_copy(around(zi, d, zs)).start()
+
+    for d in range(1, zs + 1):
+        z = around(zi, d, zs)
+        q_part[z] = project(z, c)
     share_cols = pl.ds(pl.multiple_of(t * share, share), share)
     hidden = ALPHA * tokens[:, share_cols].astype(F32)
 
-    @pl.loop(1, tp)
-    def _(d):
-        b_in(lax.rem(t + d, tp)).wait_recv()
-
-    for p in range(tp):
-        hidden = hidden + b_recv[p].astype(F32)
+    @pl.loop(1, zs + 1)
+    def _(d):
+        z = around(zi, d, zs)
+        q_copy(z).wait_recv()
+        q_part[z] = q_part[z] + q_recv[z].astype(F32)
+
+        @pl.when(d < zs)
+        def _():
+            b_send[z] = q_part[z].astype(BF16)
+            b_out(z).start()
+
+    hidden = hidden + q_part[zi]
+    b_recv[zi] = jnp.zeros(b_recv.shape[1:], BF16)
+
+    @pl.loop(1, zs)
+    def _(d):
+        b_in(around(zi, d, zs)).wait_recv()
+
+    for z in range(zs):
+        hidden = hidden + b_recv[z].astype(F32)
 
     rows[t, e] = hidden.astype(rows.dtype)
 
@@ -224,9 +253,6 @@
     def p_in(z, x):
         ref, sem = block(z, 1 - c, x)
         return remote(ref, ref, p_ss.at[z, x], sem, e, mate)
-
-    def around(i, d, size):
-        return lax.rem(i + d, size)
 
     @pl.loop(1, zs)
     def _(d):
@@ -379,8 +405,9 @@
     own_sum = jnp.sum(combined, axis=1, keepdims=True)
     centred = combined - own_sum / share
     own_square = jnp.sum(centred * centred, axis=1, keepdims=True)
-    lane = lax.broadcasted_iota(jnp.int32, stats.shape[1:], 1)
-    stats[t] = jnp.where(lane == 0, own_sum, own_square)
+    lane = lax.broadcasted_iota(jnp.int32, (seqs, 128), 1)
+    flat = jnp.transpose(jnp.where(lane == 0, own_sum, own_square))[0:2, :]
+    stats[t] = jnp.concatenate([flat, jnp.zeros((2, 128 - seqs), F32)], axis=1)
 
     def e_out(p):
         return remote(stats.at[t], stats.at[t], e_ss.at[p], e_rs.at[t], e, p)
@@ -396,18 +423,20 @@
     def _(d):
         e_in(lax.rem(t + d, tp)).wait_recv()
 
-    sums = [stats[p][:, 0:1] for p in range(tp)]
+    sums = [stats[p][0:1, :] for p in range(tp)]
     mean = functools.reduce(jnp.add, sums) / width
-    square = jnp.zeros((seqs, 1), F32)
+    square = jnp.zeros((1, 128), F32)
     for p in range(tp):
         gap = sums[p] / share - mean
-        square = square + stats[p][:, 1:2] + share * gap * gap
+        square = square + stats[p][1:2, :] + share * gap * gap
     scale = lax.rsqrt(square / width + EPSILON)
+    row = lax.broadcasted_iota(jnp.int32, (8, 128), 0)
+    tall = jnp.transpose(jnp.where(row == 0, mean, scale))
+    mean, scale = tall[:seqs, 0:1], tall[:seqs, 1:2]
     out[...] = ((combined - mean) * scale * final_gain[:, share_cols]).astype(BF16)
 
     @pl.loop(1, tp)
     def _(d):
-        b_out(lax.rem(t + d, tp)).wait_send()
         e_out(lax.rem(t + d, tp)).wait_send()
 
     @pl.loop(0, zs)
@@ -416,9 +445,11 @@
 
         @pl.when(d > 0)
         def _():
+            b_out(z).wait_send()
             z_out(z).wait_send()
             f_out(z).wait_send()
 
+        q_copy(z).wait_send()
         pair_copy(z).wait_send()
 
         @pl.loop(0, ep)
@@ -439,7 +470,6 @@
 ):
     tp = lax.axis_size("tp")
     ep = lax.axis_size("ep")
-    n = ep * tp
     seqs, width = tokens.shape
     dk, dv = old_state.shape[1:]
     heads = query_weight.shape[1] // dk
@@ -507,8 +537,11 @@
             pltpu.VMEM(glu_weight.shape[1:], BF16),
             pltpu.VMEM(linear_weight.shape[1:], BF16),
             pltpu.VMEM(down_weight.shape[1:], BF16),
-            pltpu.VMEM((tp, seqs, share), BF16),
-            pltpu.VMEM((tp, seqs, share), BF16),
+            pltpu.VMEM((zs, seqs, share), F32),
+            pltpu.VMEM((zs, seqs, share), BF16),
+            pltpu.VMEM((zs, seqs, share), BF16),
+            pltpu.VMEM((zs, seqs, share), BF16),
+            pltpu.VMEM((zs, seqs, share), BF16),
             pltpu.VMEM((tp, ep, seqs, share), BF16),
             pltpu.VMEM((tp, ep, seqs, share), BF16),
             pltpu.VMEM((zs, ep * seqs, share), F32),
@@ -518,10 +551,12 @@
             pltpu.VMEM((zs, ep, seqs, share), BF16),
             pltpu.VMEM((zs, seqs, share), BF16),
             pltpu.VMEM((zs, seqs, share), BF16),
-            pltpu.VMEM((tp, seqs, 128), F32),
+            pltpu.VMEM((tp, 2, 128), F32),
             dma((3,)),
-            dma((tp,)),
-            dma((tp,)),
+            dma((zs,)),
+            dma((zs,)),
+            dma((zs,)),
+            dma((zs,)),
             dma((zs,)),
             dma((zs, ep)),
             dma((zs, ep)),

time: 47.6 us -> 46.1 us (0.968)
  Pallas kernels: 46 us -> 44.5 us
    pallas_call x1, Pallas kernels: 33.9 us -> 32.3 us  [per_device(): pl.pallas_call(functools.partial(expert_kernel, ep, tp), out_shape=jax.Sh...]
where the time goes in v4:
time: 46.1 us; the launch traced here: 45.9 us
  Pallas kernels  44.5 us (97%)
  between operations  0.77 us (2%)
  local copies, waits for them, and re-layouts  0.65 us (1%)
    pallas_call x1, Pallas kernels, per_device(): pl.pallas_call(functools.partial(expert_kernel, ep, tp), out_shape=jax.Sh...  32.3 us
    pallas_call x1, Pallas kernels, per_device(): pl.pallas_call(functools.partial(project_kernel, tp, heads, dk), out_shap...  9.54 us
    pallas_call x1, Pallas kernels, per_device(): pl.pallas_call(state_kernel, out_shape=(jax.ShapeDtypeStruct(old_state.sh...  2.6 us

profile of v4, /device:TPU:0, one launch (start us, length us, event | category | flops | bytes accessed | tf_op | source)
XLA Modules:
  0.0 45.9 jit_solution(14132803700729455243)
XLA Ops:
  0.6 0.0 copy-start
  0.6 9.5 %project.1 = (f32[256,128]{1,0:T(8,128)S(1)}, f32[16,256]{1,0:T(8,128)S(1)}) custom-call(bf16[16,4096]{1,0:T(8,128)(2,1)} %tokens.1, bf16[512,1024]{1,0:T(8,128)(2,1)} %wq.1, bf16[512,1024]{1,0:T(8,128)(2,1)} %wk.1, bf16[4096,256]{1,0:T(8,128)(2,1)} %wv.1, bf16[16,4096]{1,0:T(8,128)(2,1)} %bitcast.10, f32[16,1024]{1,0:T(8,128)} %up_h.1, f32[1,1024]{1,0:T(1,128)} %bitcast.11), custom_call_target="tpu_custom_call" | custom-call | tf_op jit(solution)/shard_map/project/pallas_call | solution.py:484
  10.2 0.0 copy-done
  10.2 0.0 copy-start.1
  10.2 0.0 copy-start.2
  10.2 0.0 copy-start.3
  10.2 0.0 copy-start.4
  10.3 0.0 copy-start.5
  10.3 0.0 copy-start.6
  10.3 2.6 %state.1 = (f32[16,256,256]{2,1,0:T(8,128)}, bf16[16,256]{1,0:T(8,128)(2,1)S(1)}) custom-call(f32[256,128]{1,0:T(8,128)S(1)} %get-tuple-element.6.pack, f32[16,256]{1,0:T(8,128)S(1)} %get-tuple-element.7.values, f32[16,256,256]{2,1,0:T(8,128)S(1)} %copy-done), custom_call_target="tpu_custom_call" | custom-call | tf_op jit(solution)/shard_map/state/pallas_call | solution.py:515
  12.9 0.0 copy-done.1
  12.9 0.0 copy-done.2
  12.9 0.0 copy-done.3
  12.9 0.0 copy-done.4
  12.9 0.0 copy-done.5
  12.9 0.0 copy-done.6
  12.9 32.3 %experts.1 = bf16[16,512]{1,0:T(8,128)(2,1)S(1)} custom-call(bf16[16,4096]{1,0:T(8,128)(2,1)S(1)} %copy-done.2, bf16[16,256]{1,0:T(8,128)(2,1)S(1)} %get-tuple-element.8.mixed, f32[1,4096]{1,0:T(1,128)S(1)} %bitcast.7, f32[1,4096]{1,0:T(1,128)S(1)} %bitcast.8, s32[2,16]{1,0:T(2,128)S(1)} %bitcast.9, bf16[4,4096]{1,0:T(4,128)(2,1)S(1)} %bitcast.6, ...), custom_call_target="tpu_custom_call" | custom-call | tf_op jit(solution)/shard_map/experts/pallas_call | solution.py:531
  45.3 0.6 %copy.19 = bf16[16,512]{1,0:T(8,128)(2,1)} copy(bf16[16,512]{1,0:T(8,128)(2,1)S(1)} %experts.1) | data formatting | bytes 32768
Async XLA Ops:
  0.6 9.6 %copy-start = (f32[16,256,256]{2,1,0:T(8,128)S(1)}, f32[16,256,256]{2,1,0:T(8,128)}, u32[]{:S(2)}) copy-start(f32[16,256,256]{2,1,0:T(8,128)} %old.1) | copy-start | bytes 12582916
  10.2 2.7 %copy-start.1 = (bf16[256,4096]{1,0:T(8,128)(2,1)S(1)}, bf16[256,4096]{1,0:T(8,128)(2,1)}, u32[]{:S(2)}) copy-start(bf16[256,4096]{1,0:T(8,128)(2,1)} %wo.1) | copy-start | bytes 6291460
  10.2 2.7 %copy-start.2 = (bf16[16,4096]{1,0:T(8,128)(2,1)S(1)}, bf16[16,4096]{1,0:T(8,128)(2,1)}, u32[]{:S(2)}) copy-start(bf16[16,4096]{1,0:T(8,128)(2,1)} %tokens.1) | copy-start | bytes 393220
  10.2 2.7 %copy-start.3 = (bf16[4096,4]{0,1:T(4,128)(2,1)S(1)}, bf16[4096,4]{0,1:T(4,128)(2,1)}, u32[]{:S(2)}) copy-start(bf16[4096,4]{0,1:T(4,128)(2,1)} %param.26) | copy-start | bytes 98308
  10.2 2.7 %copy-start.4 = (f32[4096]{0:T(1024)S(1)}, f32[4096]{0:T(1024)}, u32[]{:S(2)}) copy-start(f32[4096]{0:T(1024)} %param.25) | copy-start | bytes 49156
  10.3 2.7 %copy-start.5 = (f32[4096]{0:T(1024)S(1)}, f32[4096]{0:T(1024)}, u32[]{:S(2)}) copy-start(f32[4096]{0:T(1024)} %param.31) | copy-start | bytes 49156
  10.3 2.7 %copy-start.6 = (s32[16,2]{0,1:T(2,128)S(1)}, s32[16,2]{0,1:T(2,128)}, u32[]{:S(2)}) copy-start(s32[16,2]{0,1:T(2,128)} %param.27) | copy-start | bytes 388

commit v5 on v4

--- a/solution.py
+++ b/solution.py
@@ -45,7 +45,7 @@
     group = tp // heads
     barrier = pltpu.get_barrier_semaphore()
 
-    @pl.loop(1, tp)
+    @pl.loop(1, tp, unroll=True)
     def _(d):
         pl.semaphore_signal(
             barrier, inc=1, device_id={"tp": lax.rem(me + d, tp)}, device_id_type=MESH
@@ -80,7 +80,7 @@
             device_id_type=MESH,
         )
 
-    @pl.loop(1, tp)
+    @pl.loop(1, tp, unroll=True)
     def _(d):
         copy_to(lax.rem(me + d, tp)).start()
 
@@ -101,7 +101,7 @@
     loads[6].wait()
     values_out[...] = mm(tokens[...], wv_v[...]).astype(BF16).astype(F32)
 
-    @pl.loop(1, tp)
+    @pl.loop(1, tp, unroll=True)
     def _(d):
         copy_from(lax.rem(me + d, tp)).wait_recv()
 
@@ -113,7 +113,7 @@
     pack = jnp.concatenate([decay, total, jnp.zeros((pad, dk), F32)], axis=0)
     pack_out[...] = jnp.transpose(pack)
 
-    @pl.loop(1, tp)
+    @pl.loop(1, tp, unroll=True)
     def _(d):
         copy_to(lax.rem(me + d, tp)).wait_send()
 
@@ -155,13 +155,13 @@
         load.start()
     barrier = pltpu.get_barrier_semaphore()
 
-    @pl.loop(1, tp)
+    @pl.loop(1, tp, unroll=True)
     def _(d):
         pl.semaphore_signal(
             barrier, inc=1, device_id={"ep": e, "tp": lax.rem(t + d, tp)}, device_id_type=MESH
         )
 
-    @pl.loop(1, ep)
+    @pl.loop(1, ep, unroll=True)
     def _(d):
         pl.semaphore_signal(
             barrier, inc=1, device_id={"ep": lax.rem(e + d, ep), "tp": t}, device_id_type=MESH
@@ -194,7 +194,7 @@
         q_send[z] = project(z, 1 - c).astype(BF16)
     pl.semaphore_wait(barrier, tp + ep - 2)
 
-    @pl.loop(1, zs + 1)
+    @pl.loop(1, zs + 1, unroll=True)
     def _(d):
         q_copy(around(zi, d, zs)).start()
 
@@ -204,7 +204,7 @@
     share_cols = pl.ds(pl.multiple_of(t * share, share), share)
     hidden = ALPHA * tokens[:, share_cols].astype(F32)
 
-    @pl.loop(1, zs + 1)
+    @pl.loop(1, zs + 1, unroll=True)
     def _(d):
         z = around(zi, d, zs)
         q_copy(z).wait_recv()
@@ -218,7 +218,7 @@
     hidden = hidden + q_part[zi]
     b_recv[zi] = jnp.zeros(b_recv.shape[1:], BF16)
 
-    @pl.loop(1, zs)
+    @pl.loop(1, zs, unroll=True)
     def _(d):
         b_in(around(zi, d, zs)).wait_recv()
 
@@ -254,11 +254,11 @@
         ref, sem = block(z, 1 - c, x)
         return remote(ref, ref, p_ss.at[z, x], sem, e, mate)
 
-    @pl.loop(1, zs)
+    @pl.loop(1, zs, unroll=True)
     def _(d):
         z_out(around(zi, d, zs)).start()
 
-    @pl.loop(0, zs)
+    @pl.loop(0, zs, unroll=True)
     def _(d):
         z = around(zi, d, zs)
 
@@ -266,27 +266,27 @@
         def _():
             z_in(z).wait_recv()
 
-        @pl.loop(1, ep)
+        @pl.loop(1, ep, unroll=True)
         def _(k):
             x_out(z, around(e, k, ep)).start()
 
         p_out(z, e).start()
 
-    @pl.loop(0, zs)
-    def _(d):
-        z = around(zi, d, zs)
-
-        @pl.loop(1, ep)
+    @pl.loop(0, zs, unroll=True)
+    def _(d):
+        z = around(zi, d, zs)
+
+        @pl.loop(1, ep, unroll=True)
         def _(k):
             x = around(e, k, ep)
             x_in(z, x).wait_recv()
             p_out(z, x).start()
 
-    @pl.loop(0, zs)
-    def _(d):
-        z = around(zi, d, zs)
-
-        @pl.loop(0, ep)
+    @pl.loop(0, zs, unroll=True)
+    def _(d):
+        z = around(zi, d, zs)
+
+        @pl.loop(0, ep, unroll=True)
         def _(k):
             p_in(z, around(e, k, ep)).wait_recv()
 
@@ -342,14 +342,14 @@
         z = around(zi, d, zs)
         own_part[z] = down(z, c)
 
-    @pl.loop(1, zs + 1)
+    @pl.loop(1, zs + 1, unroll=True)
     def _(d):
         z = around(zi, d, zs)
         pair_copy(z).wait_recv()
         both = (own_part[z] + pair_recv[z].astype(F32)).astype(BF16)
         d_send[z] = both.reshape(ep, seqs, share)
 
-        @pl.loop(1, ep)
+        @pl.loop(1, ep, unroll=True)
         def _(k):
             d_out(z, around(e, k, ep)).start()
 
@@ -376,11 +376,11 @@
     gates = jnp.transpose(gates)[:seqs, :]
     combined = ALPHA * normed[t, e].astype(F32)
 
-    @pl.loop(1, zs + 1)
-    def _(d):
-        z = around(zi, d, zs)
-
-        @pl.loop(1, ep)
+    @pl.loop(1, zs + 1, unroll=True)
+    def _(d):
+        z = around(zi, d, zs)
+
+        @pl.loop(1, ep, unroll=True)
         def _(k):
             d_in(z, around(e, k, ep)).wait_recv()
 
@@ -395,7 +395,7 @@
 
     f_recv[zi] = f_send[zi]
 
-    @pl.loop(1, zs)
+    @pl.loop(1, zs, unroll=True)
     def _(d):
         f_in(around(zi, d, zs)).wait_recv()
 
@@ -415,11 +415,11 @@
     def e_in(p):
         return remote(stats.at[t], stats.at[p], e_ss.at[p], e_rs.at[p], e, p)
 
-    @pl.loop(1, tp)
+    @pl.loop(1, tp, unroll=True)
     def _(d):
         e_out(lax.rem(t + d, tp)).start()
 
-    @pl.loop(1, tp)
+    @pl.loop(1, tp, unroll=True)
     def _(d):
         e_in(lax.rem(t + d, tp)).wait_recv()
 
@@ -435,11 +435,11 @@
     mean, scale = tall[:seqs, 0:1], tall[:seqs, 1:2]
     out[...] = ((combined - mean) * scale * final_gain[:, share_cols]).astype(BF16)
 
-    @pl.loop(1, tp)
+    @pl.loop(1, tp, unroll=True)
     def _(d):
         e_out(lax.rem(t + d, tp)).wait_send()
 
-    @pl.loop(0, zs)
+    @pl.loop(0, zs, unroll=True)
     def _(d):
         z = around(zi, d, zs)
 
@@ -452,7 +452,7 @@
         q_copy(z).wait_send()
         pair_copy(z).wait_send()
 
-        @pl.loop(0, ep)
+        @pl.loop(0, ep, unroll=True)
         def _(k):
             x = around(e, k, ep)
             p_out(z, x).wait_send()

time: 46.1 us -> 45.7 us (level)
  no operation moved by 1% of the time
where the time goes in v5:
time: 45.7 us; the launch traced here: 45.5 us
  Pallas kernels  44.1 us (96%)
  between operations  0.77 us (2%)
  local copies, waits for them, and re-layouts  0.65 us (1%)
    pallas_call x1, Pallas kernels, per_device(): pl.pallas_call(functools.partial(expert_kernel, ep, tp), out_shape=jax.Sh...  32 us
    pallas_call x1, Pallas kernels, per_device(): pl.pallas_call(functools.partial(project_kernel, tp, heads, dk), out_shap...  9.5 us
    pallas_call x1, Pallas kernels, per_device(): pl.pallas_call(state_kernel, out_shape=(jax.ShapeDtypeStruct(old_state.sh...  2.6 us

profile of v5, /device:TPU:0, one launch (start us, length us, event | category | flops | bytes accessed | tf_op | source)
XLA Modules:
  0.0 45.5 jit_solution(8542931962253495540)
XLA Ops:
  0.6 0.0 copy-start
  0.6 9.5 %project.1 = (f32[256,128]{1,0:T(8,128)S(1)}, f32[16,256]{1,0:T(8,128)S(1)}) custom-call(bf16[16,4096]{1,0:T(8,128)(2,1)} %tokens.1, bf16[512,1024]{1,0:T(8,128)(2,1)} %wq.1, bf16[512,1024]{1,0:T(8,128)(2,1)} %wk.1, bf16[4096,256]{1,0:T(8,128)(2,1)} %wv.1, bf16[16,4096]{1,0:T(8,128)(2,1)} %bitcast.10, f32[16,1024]{1,0:T(8,128)} %up_h.1, f32[1,1024]{1,0:T(1,128)} %bitcast.11), custom_call_target="tpu_custom_call" | custom-call | tf_op jit(solution)/shard_map/project/pallas_call | solution.py:484
  10.2 0.0 copy-done
  10.2 0.0 copy-start.1
  10.2 0.0 copy-start.2
  10.2 0.0 copy-start.3
  10.2 0.0 copy-start.4
  10.2 0.0 copy-start.5
  10.2 0.0 copy-start.6
  10.2 2.6 %state.1 = (f32[16,256,256]{2,1,0:T(8,128)}, bf16[16,256]{1,0:T(8,128)(2,1)S(1)}) custom-call(f32[256,128]{1,0:T(8,128)S(1)} %get-tuple-element.6.pack, f32[16,256]{1,0:T(8,128)S(1)} %get-tuple-element.7.values, f32[16,256,256]{2,1,0:T(8,128)S(1)} %copy-done), custom_call_target="tpu_custom_call" | custom-call | tf_op jit(solution)/shard_map/state/pallas_call | solution.py:515
  12.8 0.0 copy-done.1
  12.9 0.0 copy-done.2
  12.9 0.0 copy-done.3
  12.9 0.0 copy-done.4
  12.9 0.0 copy-done.5
  12.9 0.0 copy-done.6
  12.9 32.0 %experts.1 = bf16[16,512]{1,0:T(8,128)(2,1)S(1)} custom-call(bf16[16,4096]{1,0:T(8,128)(2,1)S(1)} %copy-done.2, bf16[16,256]{1,0:T(8,128)(2,1)S(1)} %get-tuple-element.8.mixed, f32[1,4096]{1,0:T(1,128)S(1)} %bitcast.7, f32[1,4096]{1,0:T(1,128)S(1)} %bitcast.8, s32[2,16]{1,0:T(2,128)S(1)} %bitcast.9, bf16[4,4096]{1,0:T(4,128)(2,1)S(1)} %bitcast.6, ...), custom_call_target="tpu_custom_call" | custom-call | tf_op jit(solution)/shard_map/experts/pallas_call | solution.py:531
  44.9 0.6 %copy.19 = bf16[16,512]{1,0:T(8,128)(2,1)} copy(bf16[16,512]{1,0:T(8,128)(2,1)S(1)} %experts.1) | data formatting | bytes 32768
Async XLA Ops:
  0.6 9.5 %copy-start = (f32[16,256,256]{2,1,0:T(8,128)S(1)}, f32[16,256,256]{2,1,0:T(8,128)}, u32[]{:S(2)}) copy-start(f32[16,256,256]{2,1,0:T(8,128)} %old.1) | copy-start | bytes 12582916
  10.2 2.7 %copy-start.1 = (bf16[256,4096]{1,0:T(8,128)(2,1)S(1)}, bf16[256,4096]{1,0:T(8,128)(2,1)}, u32[]{:S(2)}) copy-start(bf16[256,4096]{1,0:T(8,128)(2,1)} %wo.1) | copy-start | bytes 6291460
  10.2 2.7 %copy-start.2 = (bf16[16,4096]{1,0:T(8,128)(2,1)S(1)}, bf16[16,4096]{1,0:T(8,128)(2,1)}, u32[]{:S(2)}) copy-start(bf16[16,4096]{1,0:T(8,128)(2,1)} %tokens.1) | copy-start | bytes 393220
  10.2 2.7 %copy-start.3 = (bf16[4096,4]{0,1:T(4,128)(2,1)S(1)}, bf16[4096,4]{0,1:T(4,128)(2,1)}, u32[]{:S(2)}) copy-start(bf16[4096,4]{0,1:T(4,128)(2,1)} %param.26) | copy-start | bytes 98308
  10.2 2.7 %copy-start.4 = (f32[4096]{0:T(1024)S(1)}, f32[4096]{0:T(1024)}, u32[]{:S(2)}) copy-start(f32[4096]{0:T(1024)} %param.25) | copy-start | bytes 49156
  10.2 2.7 %copy-start.5 = (f32[4096]{0:T(1024)S(1)}, f32[4096]{0:T(1024)}, u32[]{:S(2)}) copy-start(f32[4096]{0:T(1024)} %param.31) | copy-start | bytes 49156
  10.2 2.7 %copy-start.6 = (s32[16,2]{0,1:T(2,128)S(1)}, s32[16,2]{0,1:T(2,128)}, u32[]{:S(2)}) copy-start(s32[16,2]{0,1:T(2,128)} %param.27) | copy-start | bytes 388
